TPU v7x, 256 devices: a whole 4x4x8 slice. The times are simulated.
256 devices in a mesh: sp: 64 (over z, y, core), tp: 4 (over x).
Axes of the slice: x: 4, y: 4, z: 8, core: 2. Of those that a mesh axis runs over, the one named last changes fastest.
Arguments:
- residual: bfloat16 [16384, 2048], P(('sp', 'tp')), may hold values from -6 to 6
- queries: bfloat16 [16384, 2048], P('sp', 'tp'), may hold values from -40 to 40
- key_rows: bfloat16 [16384, 1024], P('sp', 'tp'), may hold values from -40 to 40
- value_rows: bfloat16 [16384, 1024], P('sp', 'tp'), may hold values from -6 to 6
- forget_sums: float32 [16384, 16], P('sp', 'tp'), as said below
- out_weight: bfloat16 [2048, 2048], P('tp'), may hold values from -0.25 to 0.25
- norm_gain: float32 [2048], replicated, may hold values from 0.1 to 1.9
- expert_ids: int32 [16384, 4], P(('sp', 'tp')), may hold values from 0 to 63, all different within a row; in each aligned block of 64 rows (0 to 63, 64 to 127, ...) at most 8 rows name the same one
- route_weights: float32 [16384, 4], P(('sp', 'tp')), may hold values from 0.1 to 1
- expert_gate: bfloat16 [64, 2048, 384], P('sp'), may hold values from -0.125 to 0.125
- expert_up: bfloat16 [64, 2048, 384], P('sp'), may hold values from -0.125 to 0.125
- expert_down: bfloat16 [64, 384, 2048], P('sp'), may hold values from -0.3125 to 0.3125
- shared_gate: bfloat16 [2048, 384], replicated, may hold values from -0.125 to 0.125
- shared_up: bfloat16 [2048, 384], replicated, may hold values from -0.125 to 0.125
- shared_down: bfloat16 [384, 2048], replicated, may hold values from -0.3125 to 0.3125
Outputs:
- layer_out: bfloat16 [16384, 2048], P(('sp', 'tp'))
Inputs may be any that keep to these rules, and one draw needn't show every extreme that they name: `forget_sums`: each head's column never rises from one position to the next. `expert_ids`: each row names 4 different experts; among the rows of one device no expert is named more than 8 times.
All inputs are finite; a program needn't handle non-finite values.
Results may differ from a plain program's by a relative error of at most 0.014.
Values may be sent and summed in bfloat16 or wider, within the bound.
A program may use at most 128 MiB of HBM per device.

v0:
```python
import math

import jax
import jax.numpy as jnp
from jax import lax
from jax.sharding import PartitionSpec as P

HEADS = 16
KV_HEADS = 8
HEAD_DIM = 128
TOPK = 4


routed_scale = 2.5
norm_eps = 1e-06


def from_everyone(x, axis):
    copies = jnp.broadcast_to(x, (lax.axis_size(axis), *x.shape))
    return lax.all_to_all(copies, axis, split_axis=0, concat_axis=0, tiled=True)


def laid_out(blocks, dim):
    blocks = jnp.moveaxis(blocks, 0, dim)
    dims = blocks.shape
    return blocks.reshape(*dims[:dim], dims[dim] * dims[dim + 1], *dims[dim + 2 :])


def gather_directly(x, axis, dim):
    blocks = from_everyone(x, axis)
    return laid_out(blocks, dim)


def in_one_piece(arrays, axis, dim, along):
    ends, at = ([], 0)
    for a in arrays[:-1]:
        at += a.shape[along]
        ends.append(at)
    both = jnp.concatenate(arrays, axis=along)
    return tuple(jnp.split(lax.all_gather(both, axis, axis=dim, tiled=True), ends, axis=along))


def absorb_group(carried, query_group, shard_piece, sum_piece, score_scale):
    query_heads, query_sums, query_pos, last_pos = query_group
    key_piece, value_piece = shard_piece
    piece_rows = key_piece.shape[0]
    query_count, local_kv, group_size, head_size = query_heads.shape
    key_block = math.gcd(piece_rows, 1024)
    key_heads = key_piece.reshape(piece_rows, local_kv, head_size)
    value_heads = value_piece.reshape(piece_rows, local_kv, head_size)
    key_sums = sum_piece.reshape(piece_rows, local_kv, group_size).transpose(1, 2, 0)

    def update(block_start, held):
        row_max, row_sum, weighted = held
        key_part = lax.dynamic_slice_in_dim(key_heads, block_start, key_block, 0)
        value_part = lax.dynamic_slice_in_dim(value_heads, block_start, key_block, 0)
        sums_part = lax.dynamic_slice_in_dim(key_sums, block_start, key_block, 2)
        scores = (
            jnp.einsum("qhgd,khd->hgqk", query_heads, key_part, preferred_element_type=jnp.float32)
            * score_scale
        )
        scores = scores + (query_sums[:, :, :, None] - sums_part[:, :, None, :])
        key_pos = block_start + jnp.arange(key_block, dtype=jnp.int32)
        allowed = query_pos[:, None] >= key_pos[None, :]
        scores = jnp.where(allowed, scores, -jnp.inf)
        new_max = jnp.maximum(row_max, jnp.max(scores, axis=3))
        weights = jnp.exp(scores - new_max[:, :, :, None])
        factor = jnp.exp(row_max - new_max)
        row_sum = row_sum * factor + jnp.sum(weights, axis=3)
        products = jnp.einsum(
            "hgqk,khd->qhgd",
            weights.astype(jnp.bfloat16),
            value_part,
            preferred_element_type=jnp.float32,
        )
        weighted = weighted * factor.transpose(2, 0, 1)[:, :, :, None] + products
        return (new_max, row_sum, weighted)

    def one_block(block_index, held):
        block_start = block_index * key_block
        needed = block_start <= last_pos
        return lax.cond(needed, lambda inner: update(block_start, inner), lambda inner: inner, held)

    return lax.fori_loop(0, piece_rows // key_block, one_block, carried)


def finish(carried):
    row_max, row_sum, weighted = carried
    mixed = weighted / row_sum.transpose(2, 0, 1)[:, :, :, None]
    return mixed.reshape(mixed.shape[0], -1).astype(jnp.bfloat16)


def local(
    residual,
    queries,
    key_rows,
    value_rows,
    forget_sums,
    out_weight,
    norm_gain,
    expert_ids,
    route_weights,
    expert_gate,
    expert_up,
    expert_down,
    shared_gate,
    shared_up,
    shared_down,
):
    sp_count = lax.axis_size("sp")
    sp_index = lax.axis_index("sp")
    local_rows = queries.shape[0]
    local_kv = key_rows.shape[1] // HEAD_DIM
    group_size = HEADS // KV_HEADS
    score_scale = HEAD_DIM ** (-0.5)
    own_first = sp_index * local_rows
    all_sums = gather_directly(forget_sums, "sp", 0)
    positions = own_first + jnp.arange(local_rows, dtype=jnp.int32)
    groups = [
        (
            queries.reshape(queries.shape[0], local_kv, group_size, HEAD_DIM),
            forget_sums.reshape(forget_sums.shape[0], local_kv, group_size).transpose(1, 2, 0),
            positions,
            positions[-1],
        )
    ]

    def initial(query_count):
        return (
            jnp.full((local_kv, group_size, query_count), -1e30, jnp.float32),
            jnp.zeros((local_kv, group_size, query_count), jnp.float32),
            jnp.zeros((query_count, local_kv, group_size, HEAD_DIM), jnp.float32),
        )

    def absorb(states, shard_piece):
        return tuple(
            (
                absorb_group(held, query_group, shard_piece, all_sums, score_scale)
                for held, query_group in zip(states, groups)
            )
        )

    start_states = tuple((initial(query_group[0].shape[0]) for query_group in groups))
    states = absorb(start_states, in_one_piece((key_rows, value_rows), "sp", 0, 1))
    outputs = [finish(held) for held in states]
    attended = outputs[0]
    rows_out = local_rows // lax.axis_size("tp")
    token_heads = lax.all_to_all(attended, "tp", split_axis=0, concat_axis=1, tiled=True)
    branch = jnp.dot(
        token_heads,
        lax.all_gather(out_weight, "tp", axis=0, tiled=True),
        preferred_element_type=jnp.float32,
    )
    stream = (residual.astype(jnp.float32) + branch).astype(jnp.bfloat16)
    wide = lax.optimization_barrier(stream).astype(jnp.float32)
    normed = (
        wide * lax.rsqrt(jnp.mean(wide * wide, axis=1, keepdims=True) + norm_eps) * norm_gain
    ).astype(jnp.bfloat16)
    width = normed.shape[1]
    experts_here = expert_gate.shape[0]
    total_experts = experts_here * sp_count
    capacity = 2 * rows_out * TOPK // total_experts
    flat_ids = expert_ids.reshape(-1)
    assigned = flat_ids.shape[0]
    onehot = (flat_ids[:, None] == jnp.arange(total_experts, dtype=jnp.int32)[None, :]).astype(
        jnp.int32
    )
    slot_rank = jnp.sum((jnp.cumsum(onehot, axis=0) - 1) * onehot, axis=1)
    target = flat_ids * capacity + slot_rank
    slot_count = total_experts * capacity
    source = (
        jnp.full((slot_count,), assigned, jnp.int32)
        .at[target]
        .set(jnp.arange(assigned, dtype=jnp.int32))
    )
    padded = jnp.concatenate([normed, jnp.zeros((1, width), jnp.bfloat16)], axis=0)
    outgoing = padded[source // TOPK].reshape(sp_count, experts_here, capacity, width)
    arrived = lax.all_to_all(outgoing, "sp", split_axis=0, concat_axis=0, tiled=True)
    gate_part = jnp.einsum(
        "necd,edf->necf", arrived, expert_gate, preferred_element_type=jnp.float32
    )
    up_part = jnp.einsum("necd,edf->necf", arrived, expert_up, preferred_element_type=jnp.float32)
    hidden = (jax.nn.silu(gate_part) * up_part).astype(jnp.bfloat16)
    processed = jnp.einsum(
        "necf,efd->necd", hidden, expert_down, preferred_element_type=jnp.float32
    ).astype(jnp.bfloat16)
    returned = lax.all_to_all(processed, "sp", split_axis=0, concat_axis=0, tiled=True)
    results = returned.reshape(slot_count, width)
    picked = results[target].reshape(rows_out, TOPK, width).astype(jnp.float32)
    gates = route_weights / jnp.sum(route_weights, axis=1, keepdims=True) * routed_scale
    routed = jnp.sum(gates[:, :, None] * picked, axis=1)
    shared_hidden = (
        jax.nn.silu(jnp.dot(normed, shared_gate, preferred_element_type=jnp.float32))
        * jnp.dot(normed, shared_up, preferred_element_type=jnp.float32)
    ).astype(jnp.bfloat16)
    shared_out = jnp.dot(shared_hidden, shared_down, preferred_element_type=jnp.float32)
    return (wide + shared_out + routed).astype(jnp.bfloat16)


def solution(mesh):
    in_specs = (
        P(("sp", "tp"), None),
        P("sp", "tp"),
        P("sp", "tp"),
        P("sp", "tp"),
        P("sp", "tp"),
        P("tp", None),
        P(),
        P(("sp", "tp"), None),
        P(("sp", "tp"), None),
        P("sp", None, None),
        P("sp", None, None),
        P("sp", None, None),
        P(),
        P(),
        P(),
    )
    out_specs = P(("sp", "tp"), None)
    return jax.shard_map(local, mesh=mesh, in_specs=in_specs, out_specs=out_specs, check_vma=False)
```

profile of v0, /device:TPU:8, one launch (start us, length us, event | category | flops | bytes accessed | tf_op | source)
XLA Modules:
  0.0 427.4 jit_solution(19748104873882279)
XLA Ops:
  6.5 0.0 copy-start
  6.5 0.0 all-gather.3.cloned.1.call-start
  6.6 1.1 copy.48
  7.7 1.0 copy.49
  8.7 0.7 pad_maximum_fusion
  9.5 0.0 all-gather.3.cloned.1.call-update
  9.5 0.0 all-gather.5.cloned.1.call-start
  9.5 0.7 all-gather.5.cloned.1.call-update
  10.2 1.4 broadcast_in_dim.29
  11.7 12.1 %all-to-all-start = ((f32[64,256,4]{1,2,0:T(4,128)}), f32[64,256,4]{1,2,0:T(4,128)S(1)}, u32[]{:S(2)}, u32[]{:S(2)}) async-start(f32[64,256,4]{1,2,0:T(4,128)} %broadcast_in_dim.29), calls=%async_computation | async-start | bytes 524288 | tf_op jit(solution)/shard_map/all_to_all | solution.py:20
  23.8 0.0 copy-done.5
  23.8 0.0 copy-done.6
  23.8 0.1 copy.58
  23.9 0.1 eq.29
  24.0 0.1 eq.25
  24.1 0.6 slice.9
  24.8 0.0 copy-done.3
  24.8 0.1 copy.50
  24.9 0.2 copy.53
  25.1 0.6 reduce-window.6
  25.7 0.2 slice_reduce_fusion
  26.0 0.1 copy.57
  26.1 0.1 mul.106
  26.2 0.1 fusion.76
  26.3 1.4 scatter_custom_fusion
  27.7 9.7 %all-to-all-done = f32[64,256,4]{1,2,0:T(4,128)S(1)} async-done(((f32[64,256,4]{1,2,0:T(4,128)}), f32[64,256,4]{1,2,0:T(4,128)S(1)}, u32[]{:S(2)}, u32[]{:S(2)}) %all-to-all-start) | async-done | bytes 262176 | tf_op jit(solution)/shard_map/all_to_all | solution.py:20
  37.4 0.1 copy.51
  37.5 0.2 reshape_reshape.3
  37.7 82.5 %all-gather.3.cloned.1.call-done = bf16[16384,512]{0,1:T(8,128)(2,1)} async-done(((bf16[256,512]{0,1:T(8,128)(2,1)}), bf16[16384,512]{0,1:T(8,128)(2,1)}) %all-gather.3.cloned.1.call-update) | async-done | bytes 16777232 | tf_op jit(solution)/shard_map/all_gather | solution.py:40
  120.2 11.4 %fusion.89 = (bf16[16384,256]{0,1:T(8,128)(2,1)}, bf16[16384,256]{0,1:T(8,128)(2,1)}) fusion(bf16[16384,512]{0,1:T(8,128)(2,1)} %all-gather.3.cloned.1.call-done), kind=kLoop, calls=%fused_computation.94 | loop fusion | bytes 33554432 | tf_op jit(solution)/shard_map/split | solution.py:40
  131.7 12.1 %copy.52 = bf16[16384,2,128]{2,0,1:T(8,128)(2,1)} copy(bf16[16384,2,128]{0,2,1:T(8,128)(2,1)} %bitcast.147) | data formatting | bytes 16777216
  143.8 0.0 copy-start.2
  143.8 18.1 %while.18 = (s32[]{:T(128)}, f32[2,2,256]{2,1,0:T(2,128)S(1)}, f32[2,2,256]{2,1,0:T(2,128)S(1)}, f32[256,2,2,128]{0,3,2,1:T(8,128)S(1)}, s32[]{:T(128)}, /*index...) while((s32[]{:T(128)}, f32[2,2,256]{2,1,0:T(2,128)S(1)}, ...), condition=%wide.region_5.6_spmd.clone, body=%wide.region_0.5_spmd.clone.sunk | while | flops 555225344 | bytes 16163165 | solution.py:84
  144.5 6.6 %conditional.3 = ((f32[2,2,256]{2,1,0:T(2,128)S(1)}, f32[2,2,256]{2,1,0:T(2,128)S(1)}, f32[256,2,2,128]{0,3,2,1:T(8,128)S(1)})) conditional(s32[]{:T(128)} %convert_element_type.118, (f32[2,2,256]{2,1,0:T(2,128)S(1)}, f32[2,2,256]{2,1,0:T(2,128)S(1)}, f32[256,2,2,128]{0,3,2,1:T(8,128)S(1)}) %tuple.48, (s32[]{:T(128)}, s32[]{:T(128)}, ...), branch_computations={%region_1.0_spmd, %region_2.4_spmd} | conditional | flops 555225344 | bytes 16161878 | solution.py:82
  144.6 0.2 broadcast_compare_fusion
  144.8 2.3 fusion.5
  147.1 2.7 fusion.12
  149.8 1.4 fusion.4
  162.0 0.2 copy.54
  162.2 0.8 convert_element_type.63
  163.0 4.2 all-to-all-start.1
  167.2 10.6 %all-to-all-done.1 = bf16[4,64,512]{2,1,0:T(8,128)(2,1)S(1)} async-done(((bf16[4,64,512]{2,1,0:T(8,128)(2,1)}), bf16[4,64,512]{2,1,0:T(8,128)(2,1)S(1)}, u32[]{:S(2)}, u32[]{:S(2)}) %all-to-all-start.1) | async-done | bytes 262176 | tf_op jit(solution)/shard_map/all_to_all | solution.py:148
  177.8 32.3 %all-gather.5.cloned.1.call-done = bf16[2048,2048]{1,0:T(8,128)(2,1)} async-done(((bf16[512,2048]{1,0:T(8,128)(2,1)}), bf16[2048,2048]{1,0:T(8,128)(2,1)}) %all-gather.5.cloned.1.call-update) | async-done | bytes 8388624 | tf_op jit(solution)/shard_map/all_gather | solution.py:151
  210.2 0.0 copy-done.2
  210.2 5.0 %fusion.28 = bf16[64,2048]{1,0:T(8,128)(2,1)S(1)} fusion(bf16[64,2048]{1,0:T(8,128)(2,1)S(1)} %bitcast.150, bf16[2048,2048]{1,0:T(8,128)(2,1)} %all-gather.5.cloned.1.call-done, bf16[64,2048]{1,0:T(8,128)(2,1)S(1)} %copy-done.2), kind=kOutput, calls=%fused_computation.36 | convolution fusion | flops 537264128 | bytes 9175040 | tf_op jit(solution)/shard_map/dot_general | solution.py:149
  215.2 0.2 fusion.66
  215.3 0.0 copy-done.4
  215.3 0.1 fusion.68
  215.5 3.3 gather_fusion
  218.9 122.8 %all_to_all.31 = bf16[64,1,8,2048]{3,2,1,0:T(8,128)(2,1)S(1)} all-to-all(bf16[64,1,8,2048]{3,2,1,0:T(8,128)(2,1)} %bitcast.148), channel_id=1, replica_groups=mesh['sp'=64,'tp'=4] {'sp'}, dimensions={0} | all-to-all | bytes 4194304 | tf_op jit(solution)/shard_map/all_to_all | solution.py:178
  341.7 1.3 copy-done.1
  343.0 0.0 copy-done.8
  343.0 2.1 fusion.36
  345.1 0.0 copy-done
  345.1 5.9 %fusion.25 = bf16[64,1,8,2048]{3,2,1,0:T(8,128)(2,1)} fusion(bf16[1,384,2048]{2,1,0:T(8,128)(2,1)S(1)} %copy-done, bf16[1,2048,384]{2,1,0:T(8,128)(2,1)} %param.29, bf16[64,1,8,2048]{3,2,1,0:T(8,128)(2,1)} %copy-done.1, f32[64,1,8,384]{3,2,0,1:T(8,128)} %fusion.36), kind=kOutput, calls=%fused_computation.31 | convolution fusion | flops 1612840960 | bytes 8126464 | tf_op jit(solution)/shard_map/necf,efd->necd/dot_general | solution.py:184
  351.0 5.8 %all-to-all-start.3 = ((bf16[64,1,8,2048]{3,2,1,0:T(8,128)(2,1)}), bf16[64,1,8,2048]{3,2,1,0:T(8,128)(2,1)}, u32[]{:S(2)}, u32[]{:S(2)}) async-start(bf16[64,1,8,2048]{3,2,1,0:T(8,128)(2,1)} %fusion.25), calls=%async_computation.3 | async-start | bytes 4194304 | tf_op jit(solution)/shard_map/all_to_all | solution.py:187
  356.8 0.0 copy-done.7
  356.8 0.1 copy.56
  356.9 1.8 fusion.87
  358.8 49.2 %all-to-all-done.3 = bf16[64,1,8,2048]{3,2,1,0:T(8,128)(2,1)} async-done(((bf16[64,1,8,2048]{3,2,1,0:T(8,128)(2,1)}), bf16[64,1,8,2048]{3,2,1,0:T(8,128)(2,1)}, u32[]{:S(2)}, u32[]{:S(2)}) %all-to-all-start.3) | async-done | bytes 2097184 | tf_op jit(solution)/shard_map/all_to_all | solution.py:187
  407.9 4.2 gather_fusion.1
  412.2 1.7 reshape.128
  413.9 3.2 multiply_reduce_fusion
  417.1 3.4 fusion.27
  (64 shorter events, 0.5 us)
Async XLA Ops:
  6.5 338.6 %copy-start = (bf16[1,384,2048]{2,1,0:T(8,128)(2,1)S(1)}, bf16[1,384,2048]{2,1,0:T(8,128)(2,1)}, u32[]{:S(2)}) copy-start(bf16[1,384,2048]{2,1,0:T(8,128)(2,1)} %param.30) | copy-start | bytes 4718596
  6.5 17.2 %copy-start.5 = (f32[256,4]{0,1:T(4,128)S(1)}, f32[256,4]{0,1:T(4,128)}, u32[]{:S(2)}) copy-start(f32[256,4]{0,1:T(4,128)} %param.23) | copy-start | bytes 12292
  6.5 17.3 %copy-start.6 = (s32[64,4]{0,1:T(4,128)S(1)}, s32[64,4]{0,1:T(4,128)}, u32[]{:S(2)}) copy-start(s32[64,4]{0,1:T(4,128)} %param.26) | copy-start | bytes 3076
  6.5 18.2 %copy-start.3 = (bf16[256,512]{1,0:T(8,128)(2,1)S(1)}, bf16[256,512]{1,0:T(8,128)(2,1)}, u32[]{:S(2)}) copy-start(bf16[256,512]{1,0:T(8,128)(2,1)} %param.20) | copy-start | bytes 786436
  6.5 113.7 %all-gather.3.cloned.1.call-start = ((), (), s32[]{:S(2)}) async-start(), calls=%async_computation.4 | async-start | bytes 17039360 | tf_op jit(solution)/shard_map/all_gather | solution.py:40
  9.5 200.7 %all-gather.5.cloned.1.call-start = ((), (), s32[]{:S(2)}) async-start(), calls=%async_computation.5 | async-start | bytes 10485760 | tf_op jit(solution)/shard_map/all_gather | solution.py:151
  11.7 25.8 %all-to-all-start = ((f32[64,256,4]{1,2,0:T(4,128)}), f32[64,256,4]{1,2,0:T(4,128)S(1)}, u32[]{:S(2)}, u32[]{:S(2)}) async-start(f32[64,256,4]{1,2,0:T(4,128)} %broadcast_in_dim.29), calls=%async_computation | async-start | bytes 524288 | tf_op jit(solution)/shard_map/all_to_all | solution.py:20
  143.8 66.4 %copy-start.2 = (bf16[64,2048]{1,0:T(8,128)(2,1)S(1)}, bf16[64,2048]{1,0:T(8,128)(2,1)}, u32[]{:S(2)}) copy-start(bf16[64,2048]{1,0:T(8,128)(2,1)} %param.19) | copy-start | bytes 786436
  163.0 14.8 %all-to-all-start.1 = ((bf16[4,64,512]{2,1,0:T(8,128)(2,1)}), bf16[4,64,512]{2,1,0:T(8,128)(2,1)S(1)}, u32[]{:S(2)}, u32[]{:S(2)}) async-start(bf16[4,64,512]{2,1,0:T(8,128)(2,1)} %convert_element_type.63), calls=%async_computation.1 | async-start | bytes 524288 | tf_op jit(solution)/shard_map/all_to_all | solution.py:148
  210.2 5.1 %copy-start.4 = (f32[2048]{0:T(1024)S(1)}, f32[2048]{0:T(1024)}, u32[]{:S(2)}) copy-start(f32[2048]{0:T(1024)} %param.25) | copy-start | bytes 24580
  218.9 124.1 %copy-start.8 = (bf16[1,2048,384]{2,1,0:T(8,128)(2,1)S(1)}, bf16[1,2048,384]{2,1,0:T(8,128)(2,1)}, u32[]{:S(2)}) copy-start(bf16[1,2048,384]{2,1,0:T(8,128)(2,1)} %param.28) | copy-start | bytes 4718596
  341.7 1.3 copy-start.1
  351.0 5.8 %copy-start.7 = (f32[64,4]{0,1:T(4,128)S(1)}, f32[64,4]{0,1:T(4,128)}, u32[]{:S(2)}) copy-start(f32[64,4]{0,1:T(4,128)} %param.27) | copy-start | bytes 3076
  351.0 56.9 %all-to-all-start.3 = ((bf16[64,1,8,2048]{3,2,1,0:T(8,128)(2,1)}), bf16[64,1,8,2048]{3,2,1,0:T(8,128)(2,1)}, u32[]{:S(2)}, u32[]{:S(2)}) async-start(bf16[64,1,8,2048]{3,2,1,0:T(8,128)(2,1)} %fusion.25), calls=%async_computation.3 | async-start | bytes 4194304 | tf_op jit(solution)/shard_map/all_to_all | solution.py:187
Sparse Core Ops, SparseCore 0:
  10.0 110.1 all-gather.2
  122.0 88.1 all-gather.4
where the time goes:
time: 430 us; the launch traced here: 427 us
  waiting for transfers between devices  185 us (43%)
  blocking collectives  123 us (29%)
  local copies, waits for them, and re-layouts  42.2 us (10%)
  matrix products  23.2 us (5%)
  starting transfers between devices  22.2 us (5%)
  between operations  13.7 us (3%)
  loops' own time  11.5 us (3%)
  other arithmetic  6.65 us (2%)
    all_to_all x1, blocking collectives, local(): lax.all_to_all(outgoing, 'sp', split_axis=0, concat_axis=0, tiled=True)  123 us
    all_gather x1, waiting for transfers between devices, in_one_piece(): lax.all_gather(both, axis, axis=dim, tiled=True)  82.5 us
    all_to_all x1, waiting for transfers between devices, local(): lax.all_to_all(processed, 'sp', split_axis=0, concat_axis=0, tiled=True)  49.2 us
    all_gather x1, waiting for transfers between devices, local(): lax.all_gather(out_weight, 'tp', axis=0, tiled=True)  32.3 us
    unnamed x24, local copies, waits for them, and re-layouts  15.9 us
    all_to_all x1, starting transfers between devices, from_everyone(): return lax.all_to_all(copies, axis, split_axis=0, concat_axis=0, tiled=True)  12.1 us
    split x1, local copies, waits for them, and re-layouts, in_one_piece(): jnp.split(lax.all_gather(both, axis, axis=dim, tiled=True), ends, axis=al...  11.4 us
    another operation x1, loops' own time, absorb_group(): return lax.fori_loop(0, piece_rows // key_block, one_block, carried)  11.3 us
  transfers between devices with their start and end apart: 5, of which 5 were waited for; matrix products, arithmetic and copies ran while one was open for 9% of the time, Pallas kernels for 0%

commit v1 on v0

v1 whole, which is shorter than its diff:
```python
import functools
import math

import jax
import jax.numpy as jnp
from jax import lax
from jax.experimental import pallas as pl
from jax.experimental.pallas import tpu as pltpu
from jax.sharding import PartitionSpec as P

HEADS = 16
KV_HEADS = 8
HEAD_DIM = 128
TOPK = 4
MESH = pl.DeviceIdType.MESH
LOG2E = 1.4426950408889634
NEG = -1e30

routed_scale = 2.5
norm_eps = 1e-06

NZ, NY, NX = 8, 4, 4
UP_STEPS, DOWN_STEPS = 4, 3


def attention_kernel(
    q_in,
    k_in,
    v_in,
    f_in,
    w_in,
    res_ref,
    gain_ref,
    stream_ref,
    normed_ref,
    qbuf,
    fqbuf,
    kbuf,
    vbuf,
    fbuf,
    bias,
    acc,
    stats,
    obuf,
    lbuf,
    rbuf,
    lrecv,
    wcols,
    att,
    wbuf,
    q_send,
    q_recv,
    kv_send,
    kv_recv,
    o_send,
    o_recv,
    l_send,
    l_recv,
    w_send,
    w_recv,
    p_send,
    p_recv,
    local_sem,
):
    sp = lax.axis_index("sp")
    x = lax.axis_index("tp")
    z = sp // 8
    me8 = sp % 8
    y = me8 // 2
    c = me8 % 2
    zbase = z * 8

    def at_z(step, core):
        return ((z + step + NZ) % NZ) * 8 + y * 2 + core

    partner = zbase + y * 2 + (1 - c)
    xr = (x + 1) % NX
    xl = (x + NX - 1) % NX

    barrier = pltpu.get_barrier_semaphore()

    def greet_plane(i, _):
        n = i + 1
        r8, rx = n // NX, n % NX
        pl.semaphore_signal(
            barrier,
            inc=1,
            device_id=(zbase + (me8 + r8) % 8, (x + rx) % NX),
            device_id_type=MESH,
        )
        return 0

    lax.fori_loop(0, 31, greet_plane, 0)
    for step in (1, -1):
        for core in (0, 1):
            pl.semaphore_signal(
                barrier, inc=1, device_id=(at_z(step, core), x), device_id_type=MESH
            )
    pl.semaphore_wait(barrier, 35)

    def remote(src, dst, send, recv, sp_id, tp_id):
        return pltpu.make_async_remote_copy(
            src_ref=src,
            dst_ref=dst,
            send_sem=send,
            recv_sem=recv,
            device_id=(sp_id, tp_id),
            device_id_type=MESH,
        )

    kv_arrays = ((k_in, kbuf), (v_in, vbuf), (f_in, fbuf))
    first_sends = []
    for a in (2, 0, 1):
        src, dst = kv_arrays[a]
        pltpu.make_async_copy(src.at[c], dst.at[0, c], local_sem.at[a]).start()
        first_sends.append(
            remote(
                src.at[1 - c],
                dst.at[0, c],
                kv_send.at[a, 0, 0],
                kv_recv.at[a, 0, 0],
                partner,
                x,
            )
        )
        for step, slot in ((1, 1), (-1, 1 + UP_STEPS)):
            for h in (0, 1):
                first_sends.append(
                    remote(
                        src.at[h],
                        dst.at[slot, c],
                        kv_send.at[a, slot, h],
                        kv_recv.at[a, slot, c],
                        at_z(step, h),
                        x,
                    )
                )
    for copy in first_sends:
        copy.start()

    pltpu.make_async_copy(q_in.at[c], qbuf.at[me8], local_sem.at[3]).start()
    pltpu.make_async_copy(f_in.at[c], fqbuf.at[me8], local_sem.at[4]).start()
    pltpu.make_async_copy(w_in, wbuf.at[x], local_sem.at[5]).start()

    def q_copies(r):
        to = (me8 + r) % 8
        return (
            remote(f_in.at[to % 2], fqbuf.at[me8], q_send.at[1, r], q_recv.at[1, r], zbase + to, x),
            remote(q_in.at[to % 2], qbuf.at[me8], q_send.at[0, r], q_recv.at[0, r], zbase + to, x),
        )

    def start_q(i, _):
        for copy in q_copies(i + 1):
            copy.start()
        return 0

    lax.fori_loop(0, 7, start_q, 0)

    quarter = w_in.shape[0] // 4
    rows_a = pl.ds(c * 2 * quarter, quarter)
    rows_b = pl.ds(c * 2 * quarter + quarter, quarter)
    rows_half = pl.ds(c * 2 * quarter, 2 * quarter)
    across = (x + 2) % NX
    w_first = [
        remote(w_in.at[rows_a], wbuf.at[x, rows_a], w_send.at[0], w_recv.at[0], sp, xr),
        remote(w_in.at[rows_b], wbuf.at[x, rows_b], w_send.at[2], w_recv.at[2], sp, xl),
        remote(w_in.at[rows_b], wbuf.at[x, rows_b], w_send.at[1], w_recv.at[1], sp, xr),
        remote(w_in.at[rows_a], wbuf.at[x, rows_a], w_send.at[3], w_recv.at[3], sp, xl),
    ]
    for copy in w_first:
        copy.start()
    w_forward = [
        remote(wbuf.at[xl, rows_a], wbuf.at[xl, rows_a], w_send.at[4], w_recv.at[4], sp, xr),
        remote(wbuf.at[xr, rows_b], wbuf.at[xr, rows_b], w_send.at[5], w_recv.at[5], sp, xl),
    ]
    w_partner = [
        remote(wbuf.at[o, rows_half], wbuf.at[o, rows_half], p_send.at[i], p_recv.at[i], partner, x)
        for i, o in enumerate((xl, xr, across))
    ]

    acc[...] = jnp.zeros_like(acc)
    row = lax.broadcasted_iota(jnp.int32, stats.shape, 1)
    stats[...] = jnp.where(row < 2, NEG, 0.0)

    scale = HEAD_DIM ** (-0.5) * LOG2E

    def make_bias(slot):
        f0 = fbuf[slot, 0]
        base = f0[:, 0:1]
        for cc in (0, 1):
            f = f0 if cc == 0 else fbuf[slot, 1]
            b = (base - f) * LOG2E
            bias[cc] = jnp.concatenate([b] * 16, axis=0).T

    def task(slot, qb, masked):
        if masked:
            rows = lax.broadcasted_iota(jnp.int32, (256, 256), 0)
            cols = lax.broadcasted_iota(jnp.int32, (256, 256), 1)
            gap = (qb - 2 * y) * 256
        for h in (0, 1):
            q_h = qbuf[qb, h * 128 : (h + 1) * 128, :]
            delta = (fqbuf[qb, h : h + 1, 0:1] - fbuf[slot, 0, h : h + 1, 0:1]) * LOG2E
            scores = []
            for cc in (0, 1):
                s = jnp.dot(kbuf[slot, cc], q_h, preferred_element_type=jnp.float32)
                s = s * scale + bias[cc, :, h : h + 1]
                if masked:
                    s = jnp.where(rows + cc * 256 <= cols + gap, s, -jnp.inf)
                scores.append(s)
            top = jnp.max(jnp.maximum(scores[0], scores[1]), axis=0, keepdims=True)
            old = stats[qb, h : h + 1, :]
            new = jnp.maximum(old, top + delta)
            shift = new - delta
            factor = jnp.exp2(old - new)
            p = [jnp.exp2(s - shift) for s in scores]
            total = jnp.sum(p[0] + p[1], axis=0, keepdims=True)
            stats[qb, h : h + 1, :] = new
            stats[qb, 2 + h : 3 + h, :] = stats[qb, 2 + h : 3 + h, :] * factor + total
            mixed = jnp.dot(
                vbuf[slot, 0], p[0].astype(jnp.bfloat16), preferred_element_type=jnp.float32
            ) + jnp.dot(
                vbuf[slot, 1], p[1].astype(jnp.bfloat16), preferred_element_type=jnp.float32
            )
            acc[qb, h] = acc[qb, h] * factor + mixed

    def wait_first(a, slot):
        for h in (0, 1):
            remote(
                kv_arrays[a][0].at[h],
                kv_arrays[a][1].at[slot, h],
                kv_send.at[a, slot, h],
                kv_recv.at[a, slot, h],
                partner,
                x,
            ).wait_recv()

    def forward(a, slot, step):
        buf = kv_arrays[a][1]
        return remote(
            buf.at[slot],
            buf.at[slot + 1],
            kv_send.at[a, slot + 1, 0],
            kv_recv.at[a, slot + 1, 0],
            at_z(step, c),
            x,
        )

    forwards = []

    def arrive(slot, step, first, send_on):
        for a in (2, 0, 1):
            if first:
                wait_first(a, slot)
            else:
                forward(a, slot - 1, step).wait_recv()
            if send_on:
                copy = forward(a, slot, step)
                copy.start()
                forwards.append(copy)

    def absorb(slot, origin_ok):
        @pl.when(origin_ok)
        def _():
            make_bias(slot)

            def body(qb, _):
                task(slot, qb, False)
                return 0

            lax.fori_loop(0, 8, body, 0)

    for a in range(3):
        pltpu.make_async_copy(
            kv_arrays[a][0].at[c], kv_arrays[a][1].at[0, c], local_sem.at[a]
        ).wait()
        remote(
            kv_arrays[a][0].at[1 - c],
            kv_arrays[a][1].at[0, c],
            kv_send.at[a, 0, 0],
            kv_recv.at[a, 0, 0],
            partner,
            x,
        ).wait_recv()
    pltpu.make_async_copy(q_in.at[c], qbuf.at[me8], local_sem.at[3]).wait()
    pltpu.make_async_copy(f_in.at[c], fqbuf.at[me8], local_sem.at[4]).wait()
    arrive(1, 1, True, True)
    arrive(1 + UP_STEPS, -1, True, True)
    make_bias(0)

    def own(r, _):
        @pl.when(r > 0)
        def _():
            for copy in q_copies(jnp.maximum(r, 1)):
                copy.wait_recv()

        qb = (me8 + 8 - r) % 8

        @pl.when(qb // 2 >= y)
        def _():
            task(0, qb, True)

        return 0

    lax.fori_loop(0, 8, own, 0)
    w_first[0].wait_recv()
    w_forward[0].start()
    w_first[2 - 1].wait_recv()
    w_forward[1].start()
    absorb(1, z >= 1)
    absorb(5, z + 1 >= NZ)
    arrive(2, 1, False, True)
    arrive(6, -1, False, True)
    absorb(2, z >= 2)
    absorb(6, z + 2 >= NZ)
    arrive(3, 1, False, True)
    arrive(7, -1, False, False)
    w_first[2].wait_recv()
    w_partner[0].start()
    w_first[3].wait_recv()
    w_partner[1].start()
    absorb(3, z >= 3)
    absorb(7, z + 3 >= NZ)
    arrive(4, 1, False, False)
    absorb(4, z >= 4)
    w_forward[0].wait_recv()
    w_forward[1].wait_recv()
    w_partner[2].start()

    def o_copy(r8, rx):
        to = (me8 + r8) % 8
        tx = (x + rx) % NX
        return (
            remote(
                obuf.at[to, pl.ds(tx * 64, 64)],
                rbuf.at[y, :, pl.ds((x * 2 + c) * 256, 256)],
                o_send.at[r8, rx],
                o_recv.at[r8, rx],
                zbase + to,
                tx,
            ),
            remote(
                lbuf.at[to, tx // 2],
                lrecv.at[y, x * 2 + c],
                l_send.at[r8, rx],
                l_recv.at[r8, rx],
                zbase + to,
                tx,
            ),
        )

    def finish(r, _):
        r8 = 7 - r
        qb = (me8 + r8) % 8
        sums = []
        for h in (0, 1):
            total = stats[qb, 2 + h : 3 + h, :]
            some = total > 0.0
            inv = jnp.where(some, 1.0 / jnp.where(some, total, 1.0), 0.0)
            obuf[qb, :, h * 128 : (h + 1) * 128] = (acc[qb, h] * inv).T.astype(jnp.bfloat16)
            sums.append(
                jnp.where(
                    some, stats[qb, h : h + 1, :] + jnp.log2(jnp.where(some, total, 1.0)), NEG
                )
            )
        both = jnp.concatenate(sums + [jnp.zeros((6, 256), jnp.float32)], axis=0)
        lbuf[qb, 0] = both[:, :128]
        lbuf[qb, 1] = both[:, 128:]
        for rx in (2, 1, 3):
            for copy in o_copy(r8, rx):
                copy.start()

        @pl.when(r8 > 0)
        def _():
            for copy in o_copy(r8, 0):
                copy.start()

        return 0

    lax.fori_loop(0, 8, finish, 0)
    own_copies = (
        pltpu.make_async_copy(
            obuf.at[me8, pl.ds(x * 64, 64)],
            rbuf.at[y, :, pl.ds((x * 2 + c) * 256, 256)],
            local_sem.at[6],
        ),
        pltpu.make_async_copy(lbuf.at[me8, x // 2], lrecv.at[y, x * 2 + c], local_sem.at[7]),
    )
    for copy in own_copies:
        copy.start()
    for copy in own_copies:
        copy.wait()

    def wait_o(r, _):
        for copy in o_copy((r + 1) // NX, (r + 1) % NX):
            copy.wait_recv()
        return 0

    lax.fori_loop(0, 31, wait_o, 0)

    logs = [lrecv[i].reshape(64, 128) for i in range(NY)]
    top = jnp.maximum(jnp.maximum(logs[0], logs[1]), jnp.maximum(logs[2], logs[3]))
    parts = [jnp.exp2(v - top) for v in logs]
    inv = 1.0 / (parts[0] + parts[1] + parts[2] + parts[3])
    for i in range(NY):
        scaled = parts[i] * inv
        wcols[i] = jnp.concatenate([scaled, scaled], axis=0).T
    first_row = pl.multiple_of((x % 2) * 64, 64)
    shares = [wcols[i, pl.ds(first_row, 64), :] for i in range(NY)]
    for n in range(HEADS):
        lane = (n // 2) * 8 + n % 2
        cols = slice(n * 128, (n + 1) * 128)
        mixed = shares[0][:, lane : lane + 1] * rbuf[0, :, cols].astype(jnp.float32)
        for i in range(1, NY):
            mixed = mixed + shares[i][:, lane : lane + 1] * rbuf[i, :, cols].astype(jnp.float32)
        att[:, cols] = mixed.astype(jnp.bfloat16)

    pltpu.make_async_copy(w_in, wbuf.at[x], local_sem.at[5]).wait()
    for copy in w_partner:
        copy.wait_recv()

    width = w_in.shape[1]
    chunk = 256

    def project(i, total):
        cols = pl.ds(pl.multiple_of(i * chunk, chunk), chunk)
        part = jnp.dot(att[:, 0:512], wbuf[0, :, cols], preferred_element_type=jnp.float32)
        for b in range(1, NX):
            part = part + jnp.dot(
                att[:, b * 512 : (b + 1) * 512],
                wbuf[b, :, cols],
                preferred_element_type=jnp.float32,
            )
        stream = (res_ref[:, cols].astype(jnp.float32) + part).astype(jnp.bfloat16)
        stream_ref[:, cols] = stream
        wide = stream.astype(jnp.float32)
        return total + jnp.sum(wide * wide, axis=1, keepdims=True)

    total = lax.fori_loop(0, width // chunk, project, jnp.zeros((64, 1), jnp.float32))
    rate = lax.rsqrt(total * (1.0 / width) + norm_eps)
    normed_ref[...] = (stream_ref[...].astype(jnp.float32) * rate * gain_ref[...]).astype(
        jnp.bfloat16
    )

    for copy in first_sends + forwards + w_first + w_forward + w_partner:
        copy.wait_send()

    def wait_q(i, _):
        for copy in q_copies(i + 1):
            copy.wait_send()
        return 0

    lax.fori_loop(0, 7, wait_q, 0)

    def wait_sent(r, _):
        for copy in o_copy((r + 1) // NX, (r + 1) % NX):
            copy.wait_send()
        return 0

    lax.fori_loop(0, 31, wait_sent, 0)


def attention(residual, queries, key_rows, value_rows, forget_sums, out_weight, norm_gain):
    rows, width = residual.shape
    tokens = queries.shape[0]
    q_in = queries.T.reshape(2, 256, tokens)
    k_in = key_rows.reshape(tokens, 2, 128).transpose(1, 0, 2)
    v_in = value_rows.T.reshape(2, 128, tokens)
    f_in = jnp.pad(forget_sums.T.reshape(2, 2, tokens), ((0, 0), (0, 6), (0, 0)))
    bf16, f32 = jnp.bfloat16, jnp.float32
    anywhere = pl.BlockSpec(memory_space=pl.ANY)
    vmem = pl.BlockSpec(memory_space=pltpu.VMEM)
    dma = pltpu.SemaphoreType.DMA
    return pl.pallas_call(
        attention_kernel,
        out_shape=(
            jax.ShapeDtypeStruct((rows, width), bf16),
            jax.ShapeDtypeStruct((rows, width), bf16),
        ),
        in_specs=[anywhere] * 5 + [vmem] * 2,
        out_specs=(vmem, vmem),
        scratch_shapes=[
            pltpu.VMEM((8, 256, 256), bf16),
            pltpu.VMEM((8, 8, 256), f32),
            pltpu.VMEM((8, 2, 256, 128), bf16),
            pltpu.VMEM((8, 2, 128, 256), bf16),
            pltpu.VMEM((8, 2, 8, 256), f32),
            pltpu.VMEM((2, 256, 128), f32),
            pltpu.VMEM((8, 2, 128, 256), f32),
            pltpu.VMEM((8, 8, 256), f32),
            pltpu.VMEM((8, 256, 256), bf16),
            pltpu.VMEM((8, 2, 8, 128), f32),
            pltpu.VMEM((4, 64, 2048), bf16),
            pltpu.VMEM((4, 8, 8, 128), f32),
            pltpu.VMEM((4, 128, 128), f32),
            pltpu.VMEM((64, 2048), bf16),
            pltpu.VMEM((4, 512, 2048), bf16),
            dma((2, 8)),
            dma((2, 8)),
            dma((3, 8, 2)),
            dma((3, 8, 2)),
            dma((8, 4)),
            dma((8, 4)),
            dma((8, 4)),
            dma((8, 4)),
            dma((6,)),
            dma((6,)),
            dma((3,)),
            dma((3,)),
            dma((8,)),
        ],
        compiler_params=pltpu.CompilerParams(
            collective_id=0, has_side_effects=True, vmem_limit_bytes=48 * 1024 * 1024
        ),
        cost_estimate=pl.CostEstimate(
            flops=8 * 10**9, bytes_accessed=16 * 2**20, transcendentals=16 * 2**20
        ),
    )(q_in, k_in, v_in, f_in, out_weight, residual, norm_gain.reshape(1, width))


def local(
    residual,
    queries,
    key_rows,
    value_rows,
    forget_sums,
    out_weight,
    norm_gain,
    expert_ids,
    route_weights,
    expert_gate,
    expert_up,
    expert_down,
    shared_gate,
    shared_up,
    shared_down,
):
    stream, normed = attention(
        residual, queries, key_rows, value_rows, forget_sums, out_weight, norm_gain
    )
    sp_count = lax.axis_size("sp")
    rows_out = normed.shape[0]
    wide = stream.astype(jnp.float32)
    width = normed.shape[1]
    experts_here = expert_gate.shape[0]
    total_experts = experts_here * sp_count
    capacity = 2 * rows_out * TOPK // total_experts
    flat_ids = expert_ids.reshape(-1)
    assigned = flat_ids.shape[0]
    onehot = (flat_ids[:, None] == jnp.arange(total_experts, dtype=jnp.int32)[None, :]).astype(
        jnp.int32
    )
    slot_rank = jnp.sum((jnp.cumsum(onehot, axis=0) - 1) * onehot, axis=1)
    target = flat_ids * capacity + slot_rank
    slot_count = total_experts * capacity
    source = (
        jnp.full((slot_count,), assigned, jnp.int32)
        .at[target]
        .set(jnp.arange(assigned, dtype=jnp.int32))
    )
    padded = jnp.concatenate([normed, jnp.zeros((1, width), jnp.bfloat16)], axis=0)
    outgoing = padded[source // TOPK].reshape(sp_count, experts_here, capacity, width)
    arrived = lax.all_to_all(outgoing, "sp", split_axis=0, concat_axis=0, tiled=True)
    gate_part = jnp.einsum(
        "necd,edf->necf", arrived, expert_gate, preferred_element_type=jnp.float32
    )
    up_part = jnp.einsum("necd,edf->necf", arrived, expert_up, preferred_element_type=jnp.float32)
    hidden = (jax.nn.silu(gate_part) * up_part).astype(jnp.bfloat16)
    processed = jnp.einsum(
        "necf,efd->necd", hidden, expert_down, preferred_element_type=jnp.float32
    ).astype(jnp.bfloat16)
    returned = lax.all_to_all(processed, "sp", split_axis=0, concat_axis=0, tiled=True)
    results = returned.reshape(slot_count, width)
    picked = results[target].reshape(rows_out, TOPK, width).astype(jnp.float32)
    gates = route_weights / jnp.sum(route_weights, axis=1, keepdims=True) * routed_scale
    routed = jnp.sum(gates[:, :, None] * picked, axis=1)
    shared_hidden = (
        jax.nn.silu(jnp.dot(normed, shared_gate, preferred_element_type=jnp.float32))
        * jnp.dot(normed, shared_up, preferred_element_type=jnp.float32)
    ).astype(jnp.bfloat16)
    shared_out = jnp.dot(shared_hidden, shared_down, preferred_element_type=jnp.float32)
    return (wide + shared_out + routed).astype(jnp.bfloat16)


def solution(mesh):
    in_specs = (
        P(("sp", "tp"), None),
        P("sp", "tp"),
        P("sp", "tp"),
        P("sp", "tp"),
        P("sp", "tp"),
        P("tp", None),
        P(),
        P(("sp", "tp"), None),
        P(("sp", "tp"), None),
        P("sp", None, None),
        P("sp", None, None),
        P("sp", None, None),
        P(),
        P(),
        P(),
    )
    out_specs = P(("sp", "tp"), None)
    return jax.shard_map(local, mesh=mesh, in_specs=in_specs, out_specs=out_specs, check_vma=False)
```

time: 430 us -> 247 us (0.57)
  waiting for transfers between devices: 185 us -> 49.2 us
  Pallas kernels: 0 us -> 85.7 us
  blocking collectives: 123 us -> 70.3 us
  local copies, waits for them, and re-layouts: 42.2 us -> 17.6 us
  starting transfers between devices: 22.2 us -> 5.75 us
  between operations: 13.7 us -> 0.21 us
  loops' own time: 11.5 us -> 0 us
  matrix products: 23.2 us -> 13.2 us
    all_gather x2 -> x0, waiting for transfers between devices: 115 us -> none  [the longest x1 82.5 us: in_one_piece(): lax.all_gather(both, axis, axis=dim, tiled=True)]
    pallas_call x0 -> x1, Pallas kernels: none -> 85.7 us  [attention(): pl.pallas_call(attention_kernel, out_shape=(jax.ShapeDtypeStruct((rows, w...]
    all_to_all x1, blocking collectives: 123 us -> 70.3 us  [local(): lax.all_to_all(outgoing, 'sp', split_axis=0, concat_axis=0, tiled=True)]
    all_to_all x2 -> x0, waiting for transfers between devices: 20.3 us -> none  [the longest x1 10.6 us: local(): lax.all_to_all(attended, 'tp', split_axis=0, concat_axis=1, tiled=True)]
    all_to_all x2 -> x0, starting transfers between devices: 16.3 us -> none  [the longest x1 12.1 us: from_everyone(): return lax.all_to_all(copies, axis, split_axis=0, concat_axis=0, tiled=True)]
    another operation x17 -> x0, loops' own time: 11.5 us -> none  [the longest x1 11.3 us: absorb_group(): return lax.fori_loop(0, piece_rows // key_block, one_block, carried)]
    split x1 -> x0, local copies, waits for them, and re-layouts: 11.4 us -> none  [in_one_piece(): jnp.split(lax.all_gather(both, axis, axis=dim, tiled=True), ends, axis=al...]
    unnamed x24 -> x20, local copies, waits for them, and re-layouts: 15.9 us -> 4.82 us
  transfers between devices with their start and end apart: 5 -> 1, of which waited for: 5 -> 1; matrix products, arithmetic and copies ran while one was open for 9% -> 1% of each run, Pallas kernels for 0% -> 0%
where the time goes in v1:
time: 247 us
  Pallas kernels  85.7 us (35%)
  blocking collectives  70.3 us (28%)
  waiting for transfers between devices  49.2 us (20%)
  local copies, waits for them, and re-layouts  17.6 us (7%)
  matrix products  13.2 us (5%)
  starting transfers between devices  5.75 us (2%)
  other arithmetic  4.68 us (2%)
    pallas_call x1, Pallas kernels, attention(): pl.pallas_call(attention_kernel, out_shape=(jax.ShapeDtypeStruct((rows, w...  85.7 us
    all_to_all x1, blocking collectives, local(): lax.all_to_all(outgoing, 'sp', split_axis=0, concat_axis=0, tiled=True)  70.3 us
    all_to_all x1, waiting for transfers between devices, local(): lax.all_to_all(processed, 'sp', split_axis=0, concat_axis=0, tiled=True)  49.2 us
    dot_general x1, matrix products, local(): jnp.einsum('necf,efd->necd', hidden, expert_down, preferred_element_type=...  5.93 us
    all_to_all x1, starting transfers between devices, local(): lax.all_to_all(processed, 'sp', split_axis=0, concat_axis=0, tiled=True)  5.75 us
  transfers between devices with their start and end apart: 1, of which 1 were waited for; matrix products, arithmetic and copies ran while one was open for 1% of the time, Pallas kernels for 0%

profile of v1, /device:TPU:8, one launch (start us, length us, event | category | flops | bytes accessed | tf_op | source)
XLA Modules:
  0.0 246.7 jit_solution(16416701993133002357)
XLA Ops:
  0.0 0.0 copy-start
  0.0 0.0 copy-start.5
  0.0 0.0 copy-start.7
  0.0 0.0 copy-start.3
  0.0 0.0 copy-start.2
  0.0 0.9 copy.34
  0.9 0.1 eq.29
  1.0 0.1 eq.25
  1.2 0.7 broadcast_multiply_fusion
  1.9 0.6 reduce-window.6
  2.5 0.2 slice_reduce_fusion
  2.7 0.1 copy.33
  2.8 0.1 mul.54
  2.9 0.1 fusion.47
  3.0 1.4 scatter_custom_fusion
  4.5 1.1 copy.28
  5.6 1.0 copy.29
  6.6 0.1 copy.30
  6.7 0.0 copy-done.5
  6.7 0.1 copy.31
  6.8 0.0 copy-done.7
  6.8 0.0 copy-done.3
  6.9 0.0 copy-done.2
  6.9 0.0 copy-start.1
  6.9 1.6 copy-done.1
  8.5 85.7 %shard_map.145 = (bf16[64,2048]{1,0:T(8,128)(2,1)S(1)}, bf16[64,2048]{1,0:T(8,128)(2,1)S(1)}) custom-call(bf16[2,256,256]{2,1,0:T(8,128)(2,1)S(1)} %bitcast.107, bf16[2,256,128]{2,1,0:T(8,128)(2,1)S(1)} %bitcast.108, bf16[2,128,256]{2,1,0:T(8,128)(2,1)S(1)} %bitcast.109, f32[2,8,256]{2,1,0:T(8,128)S(1)} %pad.5.f_in, bf16[512,2048]{1,0:T(8,128)(2,1)S(1)} %copy-done.1, ...), custom_call_target="tpu_custom_call" | custom-call | flops 8000000000 | bytes 16777216 | tf_op jit(solution)/shard_map/pallas_call | solution.py:473
  94.2 3.3 %gather_fusion = bf16[512,2048]{1,0:T(8,128)(2,1)} fusion(bf16[65,2048]{1,0:T(8,128)(2,1)S(1)} %concatenate.3, s32[1024]{0:T(1024)S(1)} %pad_clamp_fusion.1), kind=kCustom, calls=%fused_computation | custom fusion | bytes 4196352 | tf_op jit(solution)/shard_map/gather | solution.py:561
  97.5 0.0 copy-start.8
  97.5 70.3 %all_to_all.10 = bf16[64,1,8,2048]{3,2,1,0:T(8,128)(2,1)S(1)} all-to-all(bf16[64,1,8,2048]{3,2,1,0:T(8,128)(2,1)} %bitcast.111), channel_id=1, replica_groups=mesh['sp'=64,'tp'=4] {'sp'}, dimensions={0} | all-to-all | bytes 4194304 | tf_op jit(solution)/shard_map/all_to_all | solution.py:562
  167.9 0.0 copy-start.4
  167.9 1.3 copy-done.4
  169.2 0.0 copy-done.8
  169.2 2.1 fusion.10
  171.3 0.0 copy-done
  171.3 5.9 %fusion = bf16[64,1,8,2048]{3,2,1,0:T(8,128)(2,1)} fusion(bf16[1,384,2048]{2,1,0:T(8,128)(2,1)S(1)} %copy-done, bf16[1,2048,384]{2,1,0:T(8,128)(2,1)} %param.25, bf16[64,1,8,2048]{3,2,1,0:T(8,128)(2,1)} %copy-done.4, f32[64,1,8,384]{3,2,0,1:T(8,128)} %fusion.10), kind=kOutput, calls=%fused_computation.4 | convolution fusion | flops 1612840960 | bytes 8126464 | tf_op jit(solution)/shard_map/necf,efd->necd/dot_general | solution.py:568
  177.2 0.0 copy-start.6
  177.2 5.8 %all-to-all-start.1 = ((bf16[64,1,8,2048]{3,2,1,0:T(8,128)(2,1)}), bf16[64,1,8,2048]{3,2,1,0:T(8,128)(2,1)}, u32[]{:S(2)}, u32[]{:S(2)}) async-start(bf16[64,1,8,2048]{3,2,1,0:T(8,128)(2,1)} %fusion), calls=%async_computation.1 | async-start | bytes 4194304 | tf_op jit(solution)/shard_map/all_to_all | solution.py:571
  183.0 0.0 copy-done.6
  183.0 0.1 copy.32
  183.1 1.8 fusion.56
  184.9 49.2 %all-to-all-done.1 = bf16[64,1,8,2048]{3,2,1,0:T(8,128)(2,1)} async-done(((bf16[64,1,8,2048]{3,2,1,0:T(8,128)(2,1)}), bf16[64,1,8,2048]{3,2,1,0:T(8,128)(2,1)}, u32[]{:S(2)}, u32[]{:S(2)}) %all-to-all-start.1) | async-done | bytes 2097184 | tf_op jit(solution)/shard_map/all_to_all | solution.py:571
  234.1 4.2 %gather_fusion.1 = bf16[256,2048]{1,0:T(8,128)(2,1)S(1)} fusion(bf16[512,2048]{1,0:T(8,128)(2,1)} %bitcast.33, s32[1024]{0:T(1024)S(1)} %pad_clamp_fusion), kind=kCustom, calls=%fused_computation.1 | custom fusion | bytes 2098176 | tf_op jit(solution)/shard_map/gather | solution.py:573
  238.4 1.7 reshape.107
  240.1 3.2 %multiply_reduce_fusion = f32[64,2048]{1,0:T(8,128)S(1)} fusion(f32[64,4,2048]{2,1,0:T(4,128)} %reshape.107, f32[64,4]{1,0:T(8,128)S(1)} %copy.32), kind=kLoop, calls=%fused_computation.12 | loop fusion | flops 917504 | bytes 2622464 | tf_op jit(solution)/shard_map/reduce_sum | solution.py:575
  243.3 3.4 %fusion.2 = bf16[64,2048]{1,0:T(8,128)(2,1)} fusion(f32[64,2048]{1,0:T(8,128)S(1)} %multiply_reduce_fusion, bf16[384,2048]{1,0:T(8,128)(2,1)} %param.29, bf16[64,2048]{1,0:T(8,128)(2,1)S(1)} %get-tuple-element.8, bf16[2048,384]{1,0:T(8,128)(2,1)} %param.28, bf16[64,2048]{1,0:T(8,128)(2,1)S(1)} %get-tuple-element.7, f32[64,384]{1,0:T(8,128)S(1)} %fusion.56), kind=kOutput, calls=%fused_computation.7 | convolution fusion | flops 201998336 | bytes 4554752 | tf_op jit(solution)/shard_map/dot_general | solution.py:580
  (13 shorter events, 0.2 us)
Async XLA Ops:
  0.0 171.3 %copy-start = (bf16[1,384,2048]{2,1,0:T(8,128)(2,1)S(1)}, bf16[1,384,2048]{2,1,0:T(8,128)(2,1)}, u32[]{:S(2)}) copy-start(bf16[1,384,2048]{2,1,0:T(8,128)(2,1)} %param.26) | copy-start | bytes 4718596
  0.0 6.7 %copy-start.5 = (bf16[256,256]{1,0:T(8,128)(2,1)S(1)}, bf16[256,256]{1,0:T(8,128)(2,1)}, u32[]{:S(2)}) copy-start(bf16[256,256]{1,0:T(8,128)(2,1)} %param.18) | copy-start | bytes 393220
  0.0 6.8 %copy-start.7 = (f32[256,4]{0,1:T(4,128)S(1)}, f32[256,4]{0,1:T(4,128)}, u32[]{:S(2)}) copy-start(f32[256,4]{0,1:T(4,128)} %param.19) | copy-start | bytes 12292
  0.0 6.8 %copy-start.3 = (f32[2048]{0:T(1024)S(1)}, f32[2048]{0:T(1024)}, u32[]{:S(2)}) copy-start(f32[2048]{0:T(1024)} %param.21) | copy-start | bytes 24580
  0.0 6.8 %copy-start.2 = (bf16[64,2048]{1,0:T(8,128)(2,1)S(1)}, bf16[64,2048]{1,0:T(8,128)(2,1)}, u32[]{:S(2)}) copy-start(bf16[64,2048]{1,0:T(8,128)(2,1)} %res_ref.1) | copy-start | bytes 786436
  6.9 1.6 copy-start.1
  97.5 71.6 %copy-start.8 = (bf16[1,2048,384]{2,1,0:T(8,128)(2,1)S(1)}, bf16[1,2048,384]{2,1,0:T(8,128)(2,1)}, u32[]{:S(2)}) copy-start(bf16[1,2048,384]{2,1,0:T(8,128)(2,1)} %param.24) | copy-start | bytes 4718596
  167.9 1.3 copy-start.4
  177.2 5.8 %copy-start.6 = (f32[64,4]{0,1:T(4,128)S(1)}, f32[64,4]{0,1:T(4,128)}, u32[]{:S(2)}) copy-start(f32[64,4]{0,1:T(4,128)} %param.23) | copy-start | bytes 3076
  177.2 56.9 %all-to-all-start.1 = ((bf16[64,1,8,2048]{3,2,1,0:T(8,128)(2,1)}), bf16[64,1,8,2048]{3,2,1,0:T(8,128)(2,1)}, u32[]{:S(2)}, u32[]{:S(2)}) async-start(bf16[64,1,8,2048]{3,2,1,0:T(8,128)(2,1)} %fusion), calls=%async_computation.1 | async-start | bytes 4194304 | tf_op jit(solution)/shard_map/all_to_all | solution.py:571

commit v2 on v1

--- a/solution.py
+++ b/solution.py
@@ -1,6 +1,3 @@
-import functools
-import math
-
 import jax
 import jax.numpy as jnp
 from jax import lax
@@ -517,6 +514,379 @@
     )(q_in, k_in, v_in, f_in, out_weight, residual, norm_gain.reshape(1, width))
 
 
+def experts_kernel(
+    normed_ref,
+    stream_ref,
+    ids_ref,
+    route_ref,
+    eg_in,
+    eu_in,
+    ed_in,
+    sg_in,
+    su_in,
+    sd_in,
+    out_ref,
+    nbuf,
+    table,
+    tables,
+    sel,
+    gate,
+    sbuf,
+    xbuf,
+    obuf,
+    rbuf,
+    cin,
+    cout,
+    total,
+    eg,
+    eu,
+    ed,
+    sg,
+    su,
+    sd,
+    n_send,
+    n_recv,
+    t_send,
+    t_recv,
+    x_send,
+    x_recv,
+    r_send,
+    r_recv,
+    c_send,
+    c_recv,
+    w_sem,
+    x_sem,
+    r_sem,
+):
+    sp = lax.axis_index("sp")
+    x = lax.axis_index("tp")
+    z = sp // 8
+    me8 = sp % 8
+    zbase = z * 8
+    width = normed_ref.shape[1]
+    half = width // 2
+
+    def at_z(step):
+        return ((z + step + NZ) % NZ) * 8 + me8
+
+    barrier = pltpu.get_barrier_semaphore()
+    for r in range(1, 8):
+        for to in (zbase + (me8 + r) % 8, at_z(r)):
+            pl.semaphore_signal(barrier, inc=1, device_id=(to, x), device_id_type=MESH)
+    loads = [
+        pltpu.make_async_copy(src, dst, w_sem.at[i])
+        for i, (src, dst) in enumerate(
+            (
+                (sg_in, sg),
+                (su_in, su),
+                (sd_in, sd),
+                (eg_in.at[0], eg),
+                (eu_in.at[0], eu),
+                (ed_in.at[0], ed),
+            )
+        )
+    ]
+    for copy in loads:
+        copy.start()
+    nbuf[0, 0] = normed_ref[:, :half]
+    nbuf[0, 1] = normed_ref[:, half:]
+    pl.semaphore_wait(barrier, 14)
+
+    def remote(src, dst, send, recv, sp_id):
+        return pltpu.make_async_remote_copy(
+            src_ref=src,
+            dst_ref=dst,
+            send_sem=send,
+            recv_sem=recv,
+            device_id=(sp_id, x),
+            device_id_type=MESH,
+        )
+
+    def pass_on(slot, to_slot, hf, step):
+        return remote(
+            nbuf.at[slot, hf],
+            nbuf.at[to_slot, hf],
+            n_send.at[to_slot, hf],
+            n_recv.at[to_slot, hf],
+            at_z(step),
+        )
+
+    sent = []
+
+    def send(copy):
+        copy.start()
+        sent.append(copy)
+
+    up, down = 1, 1 + UP_STEPS
+    for hf in (0, 1):
+        send(pass_on(0, up, hf, 1))
+        send(pass_on(0, down, hf, -1))
+
+    f32, bf16 = jnp.float32, jnp.bfloat16
+    ids = ids_ref[...]
+    weights = route_ref[...]
+    gates = weights / jnp.sum(weights, axis=1, keepdims=True) * routed_scale
+    rows = ids.shape[0]
+    experts = lax.broadcasted_iota(jnp.int32, (rows, 64), 1)
+    named = jnp.zeros((rows, 64), f32)
+    shares = jnp.zeros((rows, 64), f32)
+    for k in range(TOPK):
+        hit = ids[:, k : k + 1] == experts
+        named = named + jnp.where(hit, 1.0, 0.0)
+        shares = shares + jnp.where(hit, gates[:, k : k + 1], 0.0)
+    earlier = (
+        lax.broadcasted_iota(jnp.int32, (rows, rows), 1)
+        < lax.broadcasted_iota(jnp.int32, (rows, rows), 0)
+    )
+    named = named.astype(bf16)
+    rank = jnp.dot(jnp.where(earlier, 1.0, 0.0).astype(bf16), named, preferred_element_type=f32)
+    lane = lax.broadcasted_iota(jnp.int32, (64, 1024), 1)
+    expert = lax.broadcasted_iota(jnp.int32, (64, 1024), 0)
+    spread = jnp.where(lane // 16 == expert, 1.0, 0.0).astype(bf16)
+    named_x = jnp.dot(named, spread, preferred_element_type=f32)
+    rank_x = jnp.dot(rank.astype(bf16), spread, preferred_element_type=f32)
+    share_x = jnp.dot(shares.astype(bf16), spread, preferred_element_type=f32)
+    want = (lax.broadcasted_iota(jnp.int32, (rows, 1024), 1) % 8).astype(f32)
+    filled = jnp.where(rank_x == want, named_x, 0.0)
+    token = lax.broadcasted_iota(jnp.int32, (rows, 1024), 0).astype(f32)
+    source = jnp.sum(filled * (token + 1000.0), axis=0, keepdims=True) - 1000.0
+    share = jnp.sum(filled * share_x, axis=0, keepdims=True)
+    for p in range(NZ):
+        lanes = slice(p * 128, (p + 1) * 128)
+        table[p] = jnp.concatenate(
+            [source[:, lanes], share[:, lanes], jnp.zeros((6, 128), f32)], axis=0
+        )
+    tables[z] = table[z]
+
+    def table_copy(r):
+        to = (z + r) % NZ
+        return remote(table.at[to], tables.at[z], t_send.at[r], t_recv.at[r], to * 8 + me8)
+
+    for r in range(1, NZ):
+        send(table_copy(r))
+
+    for copy in loads[:3]:
+        copy.wait()
+    n = normed_ref[...]
+    g = jnp.dot(n, sg[...], preferred_element_type=f32)
+    u = jnp.dot(n, su[...], preferred_element_type=f32)
+    hidden = (g / (1.0 + jnp.exp(-g)) * u).astype(bf16)
+    for i in range(4):
+        cols = slice(i * width // 4, (i + 1) * width // 4)
+        total[:, cols] = stream_ref[:, cols].astype(f32) + jnp.dot(
+            hidden, sd[:, cols], preferred_element_type=f32
+        )
+
+    pairs = ((1, 5), (2, 6), (3, 7), (4, 0))
+    offset = {0: 0, 1: -1, 2: -2, 3: -3, 4: -4, 5: 1, 6: 2, 7: 3}
+
+    def arrive(slot, step, send_on):
+        for hf in (0, 1):
+            pass_on(slot - 1 if slot not in (up, down) else 0, slot, hf, step).wait_recv()
+            if send_on:
+                send(pass_on(slot, slot + 1, hf, step))
+
+    def x_copy(b, r):
+        to = (me8 + r) % 8
+        return remote(sbuf.at[b, to], xbuf.at[b, me8], x_send.at[b, r], x_recv.at[b, r], zbase + to)
+
+    def r_copy(b, r):
+        to = (me8 + r) % 8
+        return remote(obuf.at[b, to], rbuf.at[b, me8], r_send.at[b, r], r_recv.at[b, r], zbase + to)
+
+    def x_own(b):
+        return pltpu.make_async_copy(sbuf.at[b, me8], xbuf.at[b, me8], x_sem.at[b])
+
+    def r_own(b):
+        return pltpu.make_async_copy(obuf.at[b, me8], rbuf.at[b, me8], r_sem.at[b])
+
+    def dispatch(b):
+        first, second = pairs[b]
+        ta = tables[(z + offset[first] + NZ) % NZ]
+        tb = tables[(z + offset[second] + NZ) % NZ]
+        lane_of = lax.broadcasted_iota(jnp.int32, (1, 128), 1) % 16
+        src = jnp.where(lane_of < 8, ta[0:1], tb[0:1] + 64.0)
+        share_row = jnp.where(lane_of < 8, ta[1:2], tb[1:2])
+        token_of = lax.broadcasted_iota(jnp.int32, (128, 128), 0).astype(f32)
+        chosen = jnp.where(token_of == src, 1.0, 0.0)
+        sel[...] = chosen.T.astype(bf16)
+        gate[b] = (chosen * share_row).astype(bf16)
+        for hf in (0, 1):
+            for i in range(2):
+                cols = slice(i * half // 2, (i + 1) * half // 2)
+                tokens = jnp.concatenate([nbuf[first, hf, :, cols], nbuf[second, hf, :, cols]], axis=0)
+                picked = jnp.dot(sel[...], tokens, preferred_element_type=f32)
+                at = hf * half + i * half // 2
+                sbuf[b, :, :, at : at + half // 2] = picked.astype(bf16).reshape(8, 16, half // 2)
+        for r in (4, 3, 5, 2, 6, 1, 7):
+            send(x_copy(b, r))
+        x_own(b).start()
+
+    def run_expert(b):
+        for r in range(1, 8):
+            x_copy(b, r).wait_recv()
+        x_own(b).wait()
+        rows_in = xbuf[b].reshape(128, width)
+        g = jnp.dot(rows_in, eg[...], preferred_element_type=f32)
+        u = jnp.dot(rows_in, eu[...], preferred_element_type=f32)
+        hidden = (g / (1.0 + jnp.exp(-g)) * u).astype(bf16)
+        for i in range(4):
+            cols = slice(i * width // 4, (i + 1) * width // 4)
+            made = jnp.dot(hidden, ed[:, cols], preferred_element_type=f32)
+            obuf[b, :, :, cols] = made.astype(bf16).reshape(8, 16, width // 4)
+
+    def give_back(b):
+        for r in (4, 3, 5, 2, 6, 1, 7):
+            send(r_copy(b, r))
+        r_own(b).start()
+
+    def need_tables(*steps):
+        for r in steps:
+            table_copy(r).wait_recv()
+
+    arrive(1, 1, True)
+    arrive(5, -1, True)
+    need_tables(1, 7)
+    dispatch(0)
+    for copy in loads[3:]:
+        copy.wait()
+    arrive(2, 1, True)
+    arrive(6, -1, True)
+    need_tables(2, 6)
+    dispatch(1)
+    run_expert(0)
+    arrive(3, 1, True)
+    arrive(7, -1, False)
+    need_tables(3, 5)
+    dispatch(2)
+    run_expert(1)
+    arrive(4, 1, False)
+    need_tables(4)
+    dispatch(3)
+    run_expert(2)
+    give_back(2)
+    run_expert(3)
+    give_back(3)
+    give_back(1)
+    give_back(0)
+
+    def chain_copy(way, place, hf):
+        return remote(
+            cout.at[way, place, hf],
+            cin.at[way, place, hf],
+            c_send.at[way, place, hf],
+            c_recv.at[way, place, hf],
+            at_z(-1 if way == 0 else 1),
+        )
+
+    for b, places in ((3, (3, None)), (2, (2, 2)), (1, (1, 1)), (0, (0, 0))):
+        for r in range(1, 8):
+            r_copy(b, r).wait_recv()
+        r_own(b).wait()
+        for hf in (0, 1):
+            cols = slice(hf * half, (hf + 1) * half)
+            part = jnp.dot(
+                gate[b], rbuf[b, :, :, cols].reshape(128, half), preferred_element_type=f32
+            )
+            for way in (0, 1):
+                mine = part[way * 64 : (way + 1) * 64]
+                place = places[way]
+                if place is None:
+                    total[:, cols] = total[:, cols] + mine
+                    continue
+                if place < (3 if way == 0 else 2):
+                    chain_copy(way, place + 1, hf).wait_recv()
+                    mine = mine + cin[way, place + 1, hf].astype(f32)
+                cout[way, place, hf] = mine.astype(bf16)
+                send(chain_copy(way, place, hf))
+    for hf in (0, 1):
+        cols = slice(hf * half, (hf + 1) * half)
+        for way in (0, 1):
+            chain_copy(way, 0, hf).wait_recv()
+        out_ref[:, cols] = (
+            total[:, cols] + cin[0, 0, hf].astype(f32) + cin[1, 0, hf].astype(f32)
+        ).astype(bf16)
+    for copy in sent:
+        copy.wait_send()
+
+
+def experts(
+    normed,
+    stream,
+    expert_ids,
+    route_weights,
+    expert_gate,
+    expert_up,
+    expert_down,
+    shared_gate,
+    shared_up,
+    shared_down,
+):
+    rows, width = normed.shape
+    hidden = expert_gate.shape[2]
+    shared = shared_gate.shape[1]
+    bf16, f32 = jnp.bfloat16, jnp.float32
+    anywhere = pl.BlockSpec(memory_space=pl.ANY)
+    vmem = pl.BlockSpec(memory_space=pltpu.VMEM)
+    dma = pltpu.SemaphoreType.DMA
+    return pl.pallas_call(
+        experts_kernel,
+        out_shape=jax.ShapeDtypeStruct((rows, width), bf16),
+        in_specs=[vmem] * 4 + [anywhere] * 6,
+        out_specs=vmem,
+        scratch_shapes=[
+            pltpu.VMEM((8, 2, rows, width // 2), bf16),
+            pltpu.VMEM((8, 8, 128), f32),
+            pltpu.VMEM((8, 8, 128), f32),
+            pltpu.VMEM((128, 128), bf16),
+            pltpu.VMEM((4, 128, 128), bf16),
+            pltpu.VMEM((4, 8, 16, width), bf16),
+            pltpu.VMEM((4, 8, 16, width), bf16),
+            pltpu.VMEM((4, 8, 16, width), bf16),
+            pltpu.VMEM((4, 8, 16, width), bf16),
+            pltpu.VMEM((2, 4, 2, rows, width // 2), bf16),
+            pltpu.VMEM((2, 4, 2, rows, width // 2), bf16),
+            pltpu.VMEM((rows, width), f32),
+            pltpu.VMEM((width, hidden), bf16),
+            pltpu.VMEM((width, hidden), bf16),
+            pltpu.VMEM((hidden, width), bf16),
+            pltpu.VMEM((width, shared), bf16),
+            pltpu.VMEM((width, shared), bf16),
+            pltpu.VMEM((shared, width), bf16),
+            dma((8, 2)),
+            dma((8, 2)),
+            dma((8,)),
+            dma((8,)),
+            dma((4, 8)),
+            dma((4, 8)),
+            dma((4, 8)),
+            dma((4, 8)),
+            dma((2, 4, 2)),
+            dma((2, 4, 2)),
+            dma((6,)),
+            dma((4,)),
+            dma((4,)),
+        ],
+        compiler_params=pltpu.CompilerParams(
+            collective_id=1, has_side_effects=True, vmem_limit_bytes=48 * 1024 * 1024
+        ),
+        cost_estimate=pl.CostEstimate(
+            flops=4 * 10**9, bytes_accessed=16 * 2**20, transcendentals=2**20
+        ),
+    )(
+        normed,
+        stream,
+        expert_ids,
+        route_weights,
+        expert_gate,
+        expert_up,
+        expert_down,
+        shared_gate,
+        shared_up,
+        shared_down,
+    )
+
+
 def local(
     residual,
     queries,
@@ -537,48 +907,18 @@
     stream, normed = attention(
         residual, queries, key_rows, value_rows, forget_sums, out_weight, norm_gain
     )
-    sp_count = lax.axis_size("sp")
-    rows_out = normed.shape[0]
-    wide = stream.astype(jnp.float32)
-    width = normed.shape[1]
-    experts_here = expert_gate.shape[0]
-    total_experts = experts_here * sp_count
-    capacity = 2 * rows_out * TOPK // total_experts
-    flat_ids = expert_ids.reshape(-1)
-    assigned = flat_ids.shape[0]
-    onehot = (flat_ids[:, None] == jnp.arange(total_experts, dtype=jnp.int32)[None, :]).astype(
-        jnp.int32
+    return experts(
+        normed,
+        stream,
+        expert_ids,
+        route_weights,
+        expert_gate,
+        expert_up,
+        expert_down,
+        shared_gate,
+        shared_up,
+        shared_down,
     )
-    slot_rank = jnp.sum((jnp.cumsum(onehot, axis=0) - 1) * onehot, axis=1)
-    target = flat_ids * capacity + slot_rank
-    slot_count = total_experts * capacity
-    source = (
-        jnp.full((slot_count,), assigned, jnp.int32)
-        .at[target]
-        .set(jnp.arange(assigned, dtype=jnp.int32))
-    )
-    padded = jnp.concatenate([normed, jnp.zeros((1, width), jnp.bfloat16)], axis=0)
-    outgoing = padded[source // TOPK].reshape(sp_count, experts_here, capacity, width)
-    arrived = lax.all_to_all(outgoing, "sp", split_axis=0, concat_axis=0, tiled=True)
-    gate_part = jnp.einsum(
-        "necd,edf->necf", arrived, expert_gate, preferred_element_type=jnp.float32
-    )
-    up_part = jnp.einsum("necd,edf->necf", arrived, expert_up, preferred_element_type=jnp.float32)
-    hidden = (jax.nn.silu(gate_part) * up_part).astype(jnp.bfloat16)
-    processed = jnp.einsum(
-        "necf,efd->necd", hidden, expert_down, preferred_element_type=jnp.float32
-    ).astype(jnp.bfloat16)
-    returned = lax.all_to_all(processed, "sp", split_axis=0, concat_axis=0, tiled=True)
-    results = returned.reshape(slot_count, width)
-    picked = results[target].reshape(rows_out, TOPK, width).astype(jnp.float32)
-    gates = route_weights / jnp.sum(route_weights, axis=1, keepdims=True) * routed_scale
-    routed = jnp.sum(gates[:, :, None] * picked, axis=1)
-    shared_hidden = (
-        jax.nn.silu(jnp.dot(normed, shared_gate, preferred_element_type=jnp.float32))
-        * jnp.dot(normed, shared_up, preferred_element_type=jnp.float32)
-    ).astype(jnp.bfloat16)
-    shared_out = jnp.dot(shared_hidden, shared_down, preferred_element_type=jnp.float32)
-    return (wide + shared_out + routed).astype(jnp.bfloat16)
 
 
 def solution(mesh):

time: 247 us -> 185 us (0.75)
  Pallas kernels: 85.7 us -> 173 us
  blocking collectives: 70.3 us -> 0 us
  waiting for transfers between devices: 49.2 us -> 0 us
  matrix products: 13.2 us -> 0 us
  local copies, waits for them, and re-layouts: 17.6 us -> 10.9 us
  starting transfers between devices: 5.75 us -> 0 us
  other arithmetic: 4.68 us -> 0 us
    pallas_call x0 -> x1, Pallas kernels: none -> 87.3 us  [experts(): pl.pallas_call(experts_kernel, out_shape=jax.ShapeDtypeStruct((rows, widt...]
    all_to_all x1 -> x0, blocking collectives: 70.3 us -> none  [local(): lax.all_to_all(outgoing, 'sp', split_axis=0, concat_axis=0, tiled=True)]
    all_to_all x1 -> x0, waiting for transfers between devices: 49.2 us -> none  [local(): lax.all_to_all(processed, 'sp', split_axis=0, concat_axis=0, tiled=True)]
    dot_general x4 -> x0, matrix products: 13.2 us -> none  [the longest x1 5.93 us: local(): jnp.einsum('necf,efd->necd', hidden, expert_down, preferred_element_type=...]
    gather x2 -> x0, local copies, waits for them, and re-layouts: 7.58 us -> none  [the longest x1 4.23 us: local(): picked = results[target].reshape(rows_out, TOPK, width).astype(jnp.float32)]
    all_to_all x1 -> x0, starting transfers between devices: 5.75 us -> none  [local(): lax.all_to_all(processed, 'sp', split_axis=0, concat_axis=0, tiled=True)]
    reduce_sum x3 -> x0, other arithmetic: 3.3 us -> none  [the longest x1 3.18 us: local(): routed = jnp.sum(gates[:, :, None] * picked, axis=1)]
    unnamed x20, local copies, waits for them, and re-layouts: 4.82 us -> 7.96 us
  transfers between devices with their start and end apart: 1 -> 0, of which waited for: 1 -> 0; matrix products, arithmetic and copies ran while one was open for 1% -> 0% of each run, Pallas kernels for 0% -> 0%
where the time goes in v2:
time: 185 us; the launch traced here: 184 us
  Pallas kernels  173 us (94%)
  local copies, waits for them, and re-layouts  10.9 us (6%)
    pallas_call x1, Pallas kernels, experts(): pl.pallas_call(experts_kernel, out_shape=jax.ShapeDtypeStruct((rows, widt...  87.3 us
    pallas_call x1, Pallas kernels, attention(): pl.pallas_call(attention_kernel, out_shape=(jax.ShapeDtypeStruct((rows, w...  85.7 us
    unnamed x20, local copies, waits for them, and re-layouts  7.96 us

profile of v2, /device:TPU:8, one launch (start us, length us, event | category | flops | bytes accessed | tf_op | source)
XLA Modules:
  0.0 183.9 jit_solution(10639101835489040407)
XLA Ops:
  0.0 1.1 copy.20
  1.1 1.0 copy.21
  2.1 0.1 copy.22
  2.2 1.0 copy.23
  3.2 0.7 reshape.18
  3.9 0.0 copy-start
  4.0 1.6 copy-done
  5.5 0.0 copy-start.4
  5.5 0.9 copy-done.4
  6.5 0.0 copy-start.5
  6.5 0.7 copy-done.5
  7.2 0.0 copy-start.6
  7.2 0.0 copy-start.7
  7.2 0.0 copy-start.1
  7.2 85.7 %shard_map.145 = (bf16[64,2048]{1,0:T(8,128)(2,1)S(1)}, bf16[64,2048]{1,0:T(8,128)(2,1)S(1)}) custom-call(bf16[2,256,256]{2,1,0:T(8,128)(2,1)S(1)} %bitcast.8, bf16[2,256,128]{2,1,0:T(8,128)(2,1)S(1)} %bitcast.9, bf16[2,128,256]{2,1,0:T(8,128)(2,1)S(1)} %bitcast.10, f32[2,8,256]{2,1,0:T(8,128)S(1)} %pad.4.f_in, bf16[512,2048]{1,0:T(8,128)(2,1)S(1)} %copy-done, ...), custom_call_target="tpu_custom_call" | custom-call | flops 8000000000 | bytes 16777216 | tf_op jit(solution)/shard_map/pallas_call | solution.py:470
  92.9 0.0 copy-done.6
  92.9 0.1 copy.24.ids_ref
  93.0 0.0 copy-done.7
  93.0 0.1 copy.25.route_ref
  93.1 0.0 copy-done.1
  93.1 0.0 copy-start.2
  93.1 1.4 copy-done.2
  94.5 0.0 copy-start.3
  94.5 1.4 copy-done.3
  95.9 87.3 %shard_map.146 = bf16[64,2048]{1,0:T(8,128)(2,1)S(1)} custom-call(bf16[64,2048]{1,0:T(8,128)(2,1)S(1)} %get-tuple-element.7.normed_ref, bf16[64,2048]{1,0:T(8,128)(2,1)S(1)} %get-tuple-element.8.stream_ref, s32[64,4]{1,0:T(8,128)S(1)} %copy.24.ids_ref, f32[64,4]{1,0:T(8,128)S(1)} %copy.25.route_ref, bf16[1,2048,384]{2,1,0:T(8,128)(2,1)S(1)} %copy-done.1, ...), custom_call_target="tpu_custom_call" | custom-call | flops 4000000000 | bytes 16777216 | tf_op jit(solution)/shard_map/pallas_call | solution.py:832
  183.2 0.7 copy.27
  (1 shorter events, 0.0 us)
Async XLA Ops:
  3.9 1.6 copy-start
  5.5 0.9 copy-start.4
  6.5 0.7 copy-start.5
  7.2 85.7 %copy-start.6 = (s32[64,4]{0,1:T(4,128)S(1)}, s32[64,4]{0,1:T(4,128)}, u32[]{:S(2)}) copy-start(s32[64,4]{0,1:T(4,128)} %param.22) | copy-start | bytes 3076
  7.2 85.8 %copy-start.7 = (f32[64,4]{0,1:T(4,128)S(1)}, f32[64,4]{0,1:T(4,128)}, u32[]{:S(2)}) copy-start(f32[64,4]{0,1:T(4,128)} %param.23) | copy-start | bytes 3076
  7.2 85.9 %copy-start.1 = (bf16[1,2048,384]{2,1,0:T(8,128)(2,1)S(1)}, bf16[1,2048,384]{2,1,0:T(8,128)(2,1)}, u32[]{:S(2)}) copy-start(bf16[1,2048,384]{2,1,0:T(8,128)(2,1)} %eg_in.1) | copy-start | bytes 4718596
  93.1 1.4 copy-start.2
  94.5 1.4 copy-start.3

commit v3 on v2

--- a/solution.py
+++ b/solution.py
@@ -22,12 +22,12 @@
 
 def attention_kernel(
     q_in,
-    k_in,
+    k_rows,
     v_in,
-    f_in,
+    f_rows,
     w_in,
-    res_ref,
-    gain_ref,
+    res_in,
+    gain_in,
     stream_ref,
     normed_ref,
     qbuf,
@@ -35,7 +35,13 @@
     kbuf,
     vbuf,
     fbuf,
+    f_in,
     bias,
+    ones,
+    held_a,
+    held_b,
+    res_ref,
+    gain_ref,
     acc,
     stats,
     obuf,
@@ -93,6 +99,19 @@
             pl.semaphore_signal(
                 barrier, inc=1, device_id=(at_z(step, core), x), device_id_type=MESH
             )
+    pltpu.make_async_copy(q_in.at[c], qbuf.at[me8], local_sem.at[3]).start()
+    pltpu.make_async_copy(w_in, wbuf.at[x], local_sem.at[5]).start()
+    pltpu.make_async_copy(res_in, res_ref, local_sem.at[8]).start()
+    pltpu.make_async_copy(gain_in, gain_ref, local_sem.at[9]).start()
+    for h in (0, 1):
+        f_in[h] = jnp.concatenate(
+            [f_rows[2 * h : 2 * h + 2, :], jnp.zeros((6, f_rows.shape[1]), jnp.float32)], axis=0
+        )
+        row = lax.broadcasted_iota(jnp.int32, (128, 256), 0)
+        ones[h] = jnp.where((row % 8 == h) & (row < 24), 1.0, 0.0).astype(jnp.bfloat16)
+    acc[...] = jnp.zeros_like(acc)
+    row = lax.broadcasted_iota(jnp.int32, stats.shape, 1)
+    stats[...] = jnp.where(row < 2, NEG, 0.0)
     pl.semaphore_wait(barrier, 35)
 
     def remote(src, dst, send, recv, sp_id, tp_id):
@@ -105,14 +124,20 @@
             device_id_type=MESH,
         )
 
-    kv_arrays = ((k_in, kbuf), (v_in, vbuf), (f_in, fbuf))
+    kv_arrays = ((k_rows, kbuf), (v_in, vbuf), (f_in, fbuf))
+
+    def own_piece(a, h):
+        if a == 0:
+            return k_rows.at[:, pl.ds(pl.multiple_of(h * 128, 128), 128)]
+        return kv_arrays[a][0].at[h]
+
     first_sends = []
     for a in (2, 0, 1):
-        src, dst = kv_arrays[a]
-        pltpu.make_async_copy(src.at[c], dst.at[0, c], local_sem.at[a]).start()
+        dst = kv_arrays[a][1]
+        pltpu.make_async_copy(own_piece(a, c), dst.at[0, c], local_sem.at[a]).start()
         first_sends.append(
             remote(
-                src.at[1 - c],
+                own_piece(a, 1 - c),
                 dst.at[0, c],
                 kv_send.at[a, 0, 0],
                 kv_recv.at[a, 0, 0],
@@ -124,7 +149,7 @@
             for h in (0, 1):
                 first_sends.append(
                     remote(
-                        src.at[h],
+                        own_piece(a, h),
                         dst.at[slot, c],
                         kv_send.at[a, slot, h],
                         kv_recv.at[a, slot, c],
@@ -135,9 +160,7 @@
     for copy in first_sends:
         copy.start()
 
-    pltpu.make_async_copy(q_in.at[c], qbuf.at[me8], local_sem.at[3]).start()
     pltpu.make_async_copy(f_in.at[c], fqbuf.at[me8], local_sem.at[4]).start()
-    pltpu.make_async_copy(w_in, wbuf.at[x], local_sem.at[5]).start()
 
     def q_copies(r):
         to = (me8 + r) % 8
@@ -175,55 +198,98 @@
         for i, o in enumerate((xl, xr, across))
     ]
 
-    acc[...] = jnp.zeros_like(acc)
-    row = lax.broadcasted_iota(jnp.int32, stats.shape, 1)
-    stats[...] = jnp.where(row < 2, NEG, 0.0)
-
     scale = HEAD_DIM ** (-0.5) * LOG2E
+    root = HEAD_DIM**0.5
 
     def make_bias(slot):
         f0 = fbuf[slot, 0]
         base = f0[:, 0:1]
         for cc in (0, 1):
-            f = f0 if cc == 0 else fbuf[slot, 1]
-            b = (base - f) * LOG2E
-            bias[cc] = jnp.concatenate([b] * 16, axis=0).T
-
-    def task(slot, qb, masked):
-        if masked:
-            rows = lax.broadcasted_iota(jnp.int32, (256, 256), 0)
-            cols = lax.broadcasted_iota(jnp.int32, (256, 256), 1)
-            gap = (qb - 2 * y) * 256
+            rest = (base - (f0 if cc == 0 else fbuf[slot, 1])) * root
+            pieces = []
+            for _ in range(3):
+                piece = rest.astype(jnp.bfloat16).astype(jnp.float32)
+                pieces.append(piece)
+                rest = rest - piece
+            pieces.append(jnp.zeros((104, 256), jnp.float32))
+            bias[slot, cc] = jnp.concatenate(pieces, axis=0).T.astype(jnp.bfloat16)
+
+    def score(slot, qb, h, cc):
+        q_h = jnp.concatenate([qbuf[qb, h * 128 : (h + 1) * 128, :], ones[h]], axis=0)
+        keys = jnp.concatenate([kbuf[slot, cc], bias[slot, cc]], axis=1)
+        return jnp.dot(keys, q_h, preferred_element_type=jnp.float32)
+
+    span = 64
+
+    def weigh(slot, qb, h, held):
+        delta = (fqbuf[qb, h : h + 1, 0:1] - fbuf[slot, 0, h : h + 1, 0:1]) * root
+        pieces = [(cc, slice(r, r + span)) for cc in (0, 1) for r in range(0, 256, span)]
+        top = None
+        for cc, part in pieces:
+            high = jnp.max(held[h, cc, part, :].reshape(span // 8, 8, 256), axis=0)
+            top = high if top is None else jnp.maximum(top, high)
+        top = jnp.max(top, axis=0, keepdims=True)
+        old = stats[qb, h : h + 1, :]
+        new = jnp.maximum(old, top + delta)
+        shift = new - delta
+        factor = jnp.exp2((old - new) * scale)
+        total = jnp.zeros((8, 256), jnp.float32)
+        p = ([], [])
+        for cc, part in pieces:
+            e = jnp.exp2((held[h, cc, part, :] - shift) * scale)
+            total = total + jnp.sum(e.reshape(span // 8, 8, 256), axis=0)
+            p[cc].append(e.astype(jnp.bfloat16))
+        total = jnp.sum(total, axis=0, keepdims=True)
+        stats[qb, h : h + 1, :] = new
+        stats[qb, 2 + h : 3 + h, :] = stats[qb, 2 + h : 3 + h, :] * factor + total
+        mixed = jnp.dot(
+            vbuf[slot, 0], jnp.concatenate(p[0], axis=0), preferred_element_type=jnp.float32
+        ) + jnp.dot(vbuf[slot, 1], jnp.concatenate(p[1], axis=0), preferred_element_type=jnp.float32)
+        acc[qb, h] = acc[qb, h] * factor + mixed
+
+    def own_task(qb):
+        rows = lax.broadcasted_iota(jnp.int32, (256, 256), 0)
+        cols = lax.broadcasted_iota(jnp.int32, (256, 256), 1)
+        gap = (qb - 2 * y) * 256
         for h in (0, 1):
-            q_h = qbuf[qb, h * 128 : (h + 1) * 128, :]
-            delta = (fqbuf[qb, h : h + 1, 0:1] - fbuf[slot, 0, h : h + 1, 0:1]) * LOG2E
-            scores = []
             for cc in (0, 1):
-                s = jnp.dot(kbuf[slot, cc], q_h, preferred_element_type=jnp.float32)
-                s = s * scale + bias[cc, :, h : h + 1]
-                if masked:
-                    s = jnp.where(rows + cc * 256 <= cols + gap, s, -jnp.inf)
-                scores.append(s)
-            top = jnp.max(jnp.maximum(scores[0], scores[1]), axis=0, keepdims=True)
-            old = stats[qb, h : h + 1, :]
-            new = jnp.maximum(old, top + delta)
-            shift = new - delta
-            factor = jnp.exp2(old - new)
-            p = [jnp.exp2(s - shift) for s in scores]
-            total = jnp.sum(p[0] + p[1], axis=0, keepdims=True)
-            stats[qb, h : h + 1, :] = new
-            stats[qb, 2 + h : 3 + h, :] = stats[qb, 2 + h : 3 + h, :] * factor + total
-            mixed = jnp.dot(
-                vbuf[slot, 0], p[0].astype(jnp.bfloat16), preferred_element_type=jnp.float32
-            ) + jnp.dot(
-                vbuf[slot, 1], p[1].astype(jnp.bfloat16), preferred_element_type=jnp.float32
-            )
-            acc[qb, h] = acc[qb, h] * factor + mixed
+                held_a[h, cc] = jnp.where(
+                    rows + cc * 256 <= cols + gap, score(0, qb, h, cc), -jnp.inf
+                )
+        use(held_a, 0, qb)
+
+    def fill(held, slot, qb):
+        for h in (0, 1):
+            for cc in (0, 1):
+                held[h, cc] = score(slot, qb, h, cc)
+
+    def use(held, slot, qb):
+        for h in (0, 1):
+            weigh(slot, qb, h, held)
+
+    def run_tasks(count, place, after=None):
+        @pl.when(count > 0)
+        def _():
+            fill(held_a, *place(0))
+
+        def pair(i, _):
+            first, second = 2 * i, 2 * i + 1
+            fill(held_b, *place(second))
+            use(held_a, *place(first))
+            if after is not None:
+                after(first)
+            fill(held_a, *place(jnp.minimum(second + 1, count - 1)))
+            use(held_b, *place(second))
+            if after is not None:
+                after(second)
+            return 0
+
+        lax.fori_loop(0, count // 2, pair, 0)
 
     def wait_first(a, slot):
         for h in (0, 1):
             remote(
-                kv_arrays[a][0].at[h],
+                own_piece(a, h),
                 kv_arrays[a][1].at[slot, h],
                 kv_send.at[a, slot, h],
                 kv_recv.at[a, slot, h],
@@ -255,23 +321,33 @@
                 copy.start()
                 forwards.append(copy)
 
-    def absorb(slot, origin_ok):
-        @pl.when(origin_ok)
+    def valid(j):
+        return jnp.where(z >= j, 1, 0) + jnp.where(z >= NZ - j, 1, 0)
+
+    def peer(i):
+        return jnp.where(i % 2 == 1, (i + 1) // 2, (8 - i // 2) % 8)
+
+    def block_of(i):
+        return (me8 + 8 - peer(i)) % 8
+
+    def wait_query(i):
+        @pl.when(i > 0)
         def _():
-            make_bias(slot)
-
-            def body(qb, _):
-                task(slot, qb, False)
-                return 0
-
-            lax.fori_loop(0, 8, body, 0)
+            for copy in q_copies(jnp.maximum(peer(i), 1)):
+                copy.wait_recv()
+
+    def own(i):
+        wait_query(i)
+        qb = block_of(i)
+
+        @pl.when(qb // 2 >= y)
+        def _():
+            own_task(qb)
 
     for a in range(3):
-        pltpu.make_async_copy(
-            kv_arrays[a][0].at[c], kv_arrays[a][1].at[0, c], local_sem.at[a]
-        ).wait()
+        pltpu.make_async_copy(own_piece(a, c), kv_arrays[a][1].at[0, c], local_sem.at[a]).wait()
         remote(
-            kv_arrays[a][0].at[1 - c],
+            own_piece(a, 1 - c),
             kv_arrays[a][1].at[0, c],
             kv_send.at[a, 0, 0],
             kv_recv.at[a, 0, 0],
@@ -280,48 +356,44 @@
         ).wait_recv()
     pltpu.make_async_copy(q_in.at[c], qbuf.at[me8], local_sem.at[3]).wait()
     pltpu.make_async_copy(f_in.at[c], fqbuf.at[me8], local_sem.at[4]).wait()
+    make_bias(0)
+
+    near = 4
+
+    def stage_a(i, _):
+        own(i)
+        return 0
+
+    lax.fori_loop(0, near, stage_a, 0)
     arrive(1, 1, True, True)
-    arrive(1 + UP_STEPS, -1, True, True)
-    make_bias(0)
-
-    def own(r, _):
-        @pl.when(r > 0)
-        def _():
-            for copy in q_copies(jnp.maximum(r, 1)):
-                copy.wait_recv()
-
-        qb = (me8 + 8 - r) % 8
-
-        @pl.when(qb // 2 >= y)
-        def _():
-            task(0, qb, True)
-
-        return 0
-
-    lax.fori_loop(0, 8, own, 0)
+    arrive(5, -1, True, True)
+    make_bias(1)
+    make_bias(5)
+
+    run_tasks(near * valid(1), lambda t: (1 + 4 * (t // near), block_of(t % near)))
+    arrive(2, 1, False, True)
+    arrive(6, -1, False, True)
+    make_bias(2)
+    make_bias(6)
     w_first[0].wait_recv()
     w_forward[0].start()
-    w_first[2 - 1].wait_recv()
+    w_first[1].wait_recv()
     w_forward[1].start()
-    absorb(1, z >= 1)
-    absorb(5, z + 1 >= NZ)
-    arrive(2, 1, False, True)
-    arrive(6, -1, False, True)
-    absorb(2, z >= 2)
-    absorb(6, z + 2 >= NZ)
+
+    lax.fori_loop(near, 8, stage_a, 0)
+    run_tasks(near * valid(1), lambda t: (1 + 4 * (t // near), block_of(near + t % near)))
     arrive(3, 1, False, True)
     arrive(7, -1, False, False)
+    make_bias(3)
+    make_bias(7)
+
+    run_tasks(8 * valid(2), lambda t: (2 + 4 * (t // 8), block_of(t % 8)))
+    arrive(4, 1, False, False)
+    make_bias(4)
     w_first[2].wait_recv()
     w_partner[0].start()
     w_first[3].wait_recv()
     w_partner[1].start()
-    absorb(3, z >= 3)
-    absorb(7, z + 3 >= NZ)
-    arrive(4, 1, False, False)
-    absorb(4, z >= 4)
-    w_forward[0].wait_recv()
-    w_forward[1].wait_recv()
-    w_partner[2].start()
 
     def o_copy(r8, rx):
         to = (me8 + r8) % 8
@@ -345,9 +417,10 @@
             ),
         )
 
-    def finish(r, _):
-        r8 = 7 - r
-        qb = (me8 + r8) % 8
+    def finish(r):
+        i = 7 - r
+        qb = block_of(i)
+        r8 = (8 - peer(i)) % 8
         sums = []
         for h in (0, 1):
             total = stats[qb, 2 + h : 3 + h, :]
@@ -356,7 +429,7 @@
             obuf[qb, :, h * 128 : (h + 1) * 128] = (acc[qb, h] * inv).T.astype(jnp.bfloat16)
             sums.append(
                 jnp.where(
-                    some, stats[qb, h : h + 1, :] + jnp.log2(jnp.where(some, total, 1.0)), NEG
+                    some, stats[qb, h : h + 1, :] * scale + jnp.log2(jnp.where(some, total, 1.0)), NEG
                 )
             )
         both = jnp.concatenate(sums + [jnp.zeros((6, 256), jnp.float32)], axis=0)
@@ -371,9 +444,28 @@
             for copy in o_copy(r8, 0):
                 copy.start()
 
+    last = jnp.where(z >= 3, 1, 0) + jnp.where(z >= 4, 1, 0) + jnp.where(z >= 5, 1, 0)
+    per_block = jnp.maximum(last, 1)
+
+    def last_place(t):
+        k = t % per_block
+        return jnp.where(k == 0, 3, jnp.where(k == 1, 4, 7)), block_of(7 - t // per_block)
+
+    def leave(t):
+        @pl.when(t % per_block == per_block - 1)
+        def _():
+            finish(t // per_block)
+
+    run_tasks(8 * last, last_place, leave)
+
+    def finish_early(r, _):
+        finish(r)
         return 0
 
-    lax.fori_loop(0, 8, finish, 0)
+    lax.fori_loop(0, jnp.where(last == 0, 8, 0), finish_early, 0)
+    w_forward[0].wait_recv()
+    w_forward[1].wait_recv()
+    w_partner[2].start()
     own_copies = (
         pltpu.make_async_copy(
             obuf.at[me8, pl.ds(x * 64, 64)],
@@ -412,6 +504,8 @@
         att[:, cols] = mixed.astype(jnp.bfloat16)
 
     pltpu.make_async_copy(w_in, wbuf.at[x], local_sem.at[5]).wait()
+    pltpu.make_async_copy(res_in, res_ref, local_sem.at[8]).wait()
+    pltpu.make_async_copy(gain_in, gain_ref, local_sem.at[9]).wait()
     for copy in w_partner:
         copy.wait_recv()
 
@@ -460,11 +554,10 @@
     rows, width = residual.shape
     tokens = queries.shape[0]
     q_in = queries.T.reshape(2, 256, tokens)
-    k_in = key_rows.reshape(tokens, 2, 128).transpose(1, 0, 2)
     v_in = value_rows.T.reshape(2, 128, tokens)
-    f_in = jnp.pad(forget_sums.T.reshape(2, 2, tokens), ((0, 0), (0, 6), (0, 0)))
     bf16, f32 = jnp.bfloat16, jnp.float32
     anywhere = pl.BlockSpec(memory_space=pl.ANY)
+    hbm = pl.BlockSpec(memory_space=pl.ANY)
     vmem = pl.BlockSpec(memory_space=pltpu.VMEM)
     dma = pltpu.SemaphoreType.DMA
     return pl.pallas_call(
@@ -473,7 +566,7 @@
             jax.ShapeDtypeStruct((rows, width), bf16),
             jax.ShapeDtypeStruct((rows, width), bf16),
         ),
-        in_specs=[anywhere] * 5 + [vmem] * 2,
+        in_specs=[anywhere, hbm, anywhere, vmem, hbm, hbm, hbm],
         out_specs=(vmem, vmem),
         scratch_shapes=[
             pltpu.VMEM((8, 256, 256), bf16),
@@ -481,7 +574,13 @@
             pltpu.VMEM((8, 2, 256, 128), bf16),
             pltpu.VMEM((8, 2, 128, 256), bf16),
             pltpu.VMEM((8, 2, 8, 256), f32),
-            pltpu.VMEM((2, 256, 128), f32),
+            pltpu.VMEM((2, 8, 256), f32),
+            pltpu.VMEM((8, 2, 256, 128), bf16),
+            pltpu.VMEM((2, 128, 256), bf16),
+            pltpu.VMEM((2, 2, 256, 256), f32),
+            pltpu.VMEM((2, 2, 256, 256), f32),
+            pltpu.VMEM((64, 2048), bf16),
+            pltpu.VMEM((1, 2048), f32),
             pltpu.VMEM((8, 2, 128, 256), f32),
             pltpu.VMEM((8, 8, 256), f32),
             pltpu.VMEM((8, 256, 256), bf16),
@@ -503,15 +602,15 @@
             dma((6,)),
             dma((3,)),
             dma((3,)),
-            dma((8,)),
+            dma((10,)),
         ],
         compiler_params=pltpu.CompilerParams(
-            collective_id=0, has_side_effects=True, vmem_limit_bytes=48 * 1024 * 1024
+            collective_id=0, has_side_effects=True, vmem_limit_bytes=66_000_000
         ),
         cost_estimate=pl.CostEstimate(
             flops=8 * 10**9, bytes_accessed=16 * 2**20, transcendentals=16 * 2**20
         ),
-    )(q_in, k_in, v_in, f_in, out_weight, residual, norm_gain.reshape(1, width))
+    )(q_in, key_rows, v_in, forget_sums.T, out_weight, residual, norm_gain.reshape(1, width))
 
 
 def experts_kernel(
@@ -764,9 +863,9 @@
     need_tables(4)
     dispatch(3)
     run_expert(2)
-    give_back(2)
     run_expert(3)
     give_back(3)
+    give_back(2)
     give_back(1)
     give_back(0)
 
@@ -826,13 +925,13 @@
     hidden = expert_gate.shape[2]
     shared = shared_gate.shape[1]
     bf16, f32 = jnp.bfloat16, jnp.float32
-    anywhere = pl.BlockSpec(memory_space=pl.ANY)
+    hbm = pl.BlockSpec(memory_space=pl.ANY)
     vmem = pl.BlockSpec(memory_space=pltpu.VMEM)
     dma = pltpu.SemaphoreType.DMA
     return pl.pallas_call(
         experts_kernel,
         out_shape=jax.ShapeDtypeStruct((rows, width), bf16),
-        in_specs=[vmem] * 4 + [anywhere] * 6,
+        in_specs=[vmem] * 4 + [hbm] * 6,
         out_specs=vmem,
         scratch_shapes=[
             pltpu.VMEM((8, 2, rows, width // 2), bf16),
@@ -868,7 +967,7 @@
             dma((4,)),
         ],
         compiler_params=pltpu.CompilerParams(
-            collective_id=1, has_side_effects=True, vmem_limit_bytes=48 * 1024 * 1024
+            collective_id=1, has_side_effects=True, vmem_limit_bytes=66_000_000
         ),
         cost_estimate=pl.CostEstimate(
             flops=4 * 10**9, bytes_accessed=16 * 2**20, transcendentals=2**20

time: 185 us -> 151 us (0.82)
  Pallas kernels: 173 us -> 143 us
  local copies, waits for them, and re-layouts: 10.9 us -> 6.54 us
    pallas_call x1, Pallas kernels: 85.7 us -> 65.8 us  [attention(): pl.pallas_call(attention_kernel, out_shape=(jax.ShapeDtypeStruct((rows, w...]
    pallas_call x1, Pallas kernels: 87.3 us -> 77.1 us  [experts(): pl.pallas_call(experts_kernel, out_shape=jax.ShapeDtypeStruct((rows, widt...]
    unnamed x20 -> x7, local copies, waits for them, and re-layouts: 7.96 us -> 3.09 us
where the time goes in v3:
time: 151 us; the launch traced here: 150 us
  Pallas kernels  143 us (95%)
  local copies, waits for them, and re-layouts  6.54 us (4%)
    pallas_call x1, Pallas kernels, experts(): pl.pallas_call(experts_kernel, out_shape=jax.ShapeDtypeStruct((rows, widt...  77.1 us
    pallas_call x1, Pallas kernels, attention(): pl.pallas_call(attention_kernel, out_shape=(jax.ShapeDtypeStruct((rows, w...  65.8 us
    unnamed x7, local copies, waits for them, and re-layouts  3.09 us

profile of v3, /device:TPU:8, one launch (start us, length us, event | category | flops | bytes accessed | tf_op | source)
XLA Modules:
  0.0 149.5 jit_solution(4559097910800217912)
XLA Ops:
  0.0 1.8 %copy.16 = bf16[512,256]{1,0:T(8,128)(2,1)} copy(bf16[512,256]{0,1:T(8,128)(2,1)} %bitcast.6) | data formatting | bytes 524288 | tf_op jit(solution)/shard_map/transpose | solution.py:556
  1.8 1.7 %copy.17 = bf16[256,256]{1,0:T(8,128)(2,1)} copy(bf16[256,256]{0,1:T(8,128)(2,1)} %bitcast.8) | data formatting | bytes 262144 | tf_op jit(solution)/shard_map/transpose | solution.py:557
  3.4 0.0 copy-start
  3.4 0.0 copy-start.1
  3.4 65.8 %shard_map.145 = (bf16[64,2048]{1,0:T(8,128)(2,1)}, bf16[64,2048]{1,0:T(8,128)(2,1)}) custom-call(bf16[2,256,256]{2,1,0:T(8,128)(2,1)} %bitcast.7, bf16[256,256]{1,0:T(8,128)(2,1)} %k_rows.1, bf16[2,128,256]{2,1,0:T(8,128)(2,1)} %bitcast.9, f32[4,256]{1,0:T(4,128)} %bitcast.11, bf16[512,2048]{1,0:T(8,128)(2,1)} %w_in.1, bf16[64,2048]{1,0:T(8,128)(2,1)} %res_in.1, ...), custom_call_target="tpu_custom_call" | custom-call | flops 8000000000 | bytes 16777216 | tf_op jit(solution)/shard_map/pallas_call | solution.py:563
  69.2 0.0 copy-done
  69.3 0.7 copy.18.ids_ref
  70.0 0.0 copy-done.1
  70.0 0.7 copy.19.route_ref
  70.7 77.1 %shard_map.146 = bf16[64,2048]{1,0:T(8,128)(2,1)} custom-call(bf16[64,2048]{1,0:T(8,128)(2,1)} %get-tuple-element.7.normed_ref, bf16[64,2048]{1,0:T(8,128)(2,1)} %get-tuple-element.8.stream_ref, s32[64,4]{1,0:T(8,128)} %copy.18.ids_ref, f32[64,4]{1,0:T(8,128)} %copy.19.route_ref, bf16[1,2048,384]{2,1,0:T(8,128)(2,1)} %eg_in.1, bf16[1,2048,384]{2,1,0:T(8,128)(2,1)} %eu_in.1, ...), custom_call_target="tpu_custom_call" | custom-call | flops 4000000000 | bytes 16777216 | tf_op jit(solution)/shard_map/pallas_call | solution.py:931
  147.8 1.7 %copy.21 = bf16[64,2048]{1,0:T(8,128)(2,1)} copy(bf16[64,2048]{1,0:T(8,128)(2,1)} %shard_map.146) | data formatting | bytes 524288
Async XLA Ops:
  3.4 65.8 %copy-start = (s32[64,4]{0,1:T(4,128)S(1)}, s32[64,4]{0,1:T(4,128)}, u32[]{:S(2)}) copy-start(s32[64,4]{0,1:T(4,128)} %param.22) | copy-start | bytes 3076
  3.4 66.5 %copy-start.1 = (f32[64,4]{0,1:T(4,128)S(1)}, f32[64,4]{0,1:T(4,128)}, u32[]{:S(2)}) copy-start(f32[64,4]{0,1:T(4,128)} %param.23) | copy-start | bytes 3076

commit v4 on v3

v4 whole, which is shorter than its diff:
```python
import jax
import jax.numpy as jnp
from jax import lax
from jax.experimental import pallas as pl
from jax.experimental.pallas import tpu as pltpu
from jax.sharding import PartitionSpec as P

HEADS = 16
KV_HEADS = 8
HEAD_DIM = 128
TOPK = 4
MESH = pl.DeviceIdType.MESH
LOG2E = 1.4426950408889634
NEG = -1e30

routed_scale = 2.5
norm_eps = 1e-06

NZ, NY, NX = 8, 4, 4
UP_STEPS, DOWN_STEPS = 4, 3


def attention_kernel(
    prepare,
    q_in,
    k_rows,
    v_in,
    f_rows,
    w_in,
    res_in,
    gain_in,
    stream_ref,
    normed_ref,
    qbuf,
    fqbuf,
    kbuf,
    vbuf,
    fbuf,
    f_in,
    bias,
    ones,
    held_a,
    held_b,
    res_ref,
    gain_ref,
    acc,
    stats,
    obuf,
    lbuf,
    rbuf,
    lrecv,
    wcols,
    att,
    wbuf,
    q_send,
    q_recv,
    kv_send,
    kv_recv,
    o_send,
    o_recv,
    l_send,
    l_recv,
    w_send,
    w_recv,
    s_send,
    s_recv,
    p_send,
    p_recv,
    local_sem,
):
    sp = lax.axis_index("sp")
    x = lax.axis_index("tp")
    z = sp // 8
    me8 = sp % 8
    y = me8 // 2
    c = me8 % 2
    zbase = z * 8

    def at_z(step, core):
        return ((z + step + NZ) % NZ) * 8 + y * 2 + core

    partner = zbase + y * 2 + (1 - c)
    xr = (x + 1) % NX
    xl = (x + NX - 1) % NX

    barrier = pltpu.get_barrier_semaphore()

    def greet_plane(i, _):
        n = i + 1
        r8, rx = n // NX, n % NX
        pl.semaphore_signal(
            barrier,
            inc=1,
            device_id=(zbase + (me8 + r8) % 8, (x + rx) % NX),
            device_id_type=MESH,
        )
        return 0

    lax.fori_loop(0, 31, greet_plane, 0)
    for step in range(2, NZ - 1):
        pl.semaphore_signal(barrier, inc=1, device_id=(at_z(step, c), x), device_id_type=MESH)
    for step in (1, -1):
        for core in (0, 1):
            pl.semaphore_signal(
                barrier, inc=1, device_id=(at_z(step, core), x), device_id_type=MESH
            )
    pltpu.make_async_copy(q_in.at[c], qbuf.at[me8], local_sem.at[3]).start()
    pltpu.make_async_copy(w_in, wbuf.at[x], local_sem.at[5]).start()
    pltpu.make_async_copy(res_in, res_ref, local_sem.at[8]).start()
    pltpu.make_async_copy(gain_in, gain_ref, local_sem.at[9]).start()
    for h in (0, 1):
        f_in[h] = jnp.concatenate(
            [f_rows[2 * h : 2 * h + 2, :], jnp.zeros((6, f_rows.shape[1]), jnp.float32)], axis=0
        )
        row = lax.broadcasted_iota(jnp.int32, (128, 256), 0)
        ones[h] = jnp.where((row % 8 == h) & (row < 24), 1.0, 0.0).astype(jnp.bfloat16)
    acc[...] = jnp.zeros_like(acc)
    row = lax.broadcasted_iota(jnp.int32, stats.shape, 1)
    stats[...] = jnp.where(row < 2, NEG, 0.0)
    pl.semaphore_wait(barrier, 40)

    def remote(src, dst, send, recv, sp_id, tp_id):
        return pltpu.make_async_remote_copy(
            src_ref=src,
            dst_ref=dst,
            send_sem=send,
            recv_sem=recv,
            device_id=(sp_id, tp_id),
            device_id_type=MESH,
        )

    kv_arrays = ((k_rows, kbuf), (v_in, vbuf), (f_in, fbuf))

    def own_piece(a, h):
        if a == 0:
            return k_rows.at[:, pl.ds(pl.multiple_of(h * 128, 128), 128)]
        return kv_arrays[a][0].at[h]

    first_sends = []
    for a in (2, 0, 1):
        dst = kv_arrays[a][1]
        pltpu.make_async_copy(own_piece(a, c), dst.at[0, c], local_sem.at[a]).start()
        first_sends.append(
            remote(
                own_piece(a, 1 - c),
                dst.at[0, c],
                kv_send.at[a, 0, 0],
                kv_recv.at[a, 0, 0],
                partner,
                x,
            )
        )
        for step, slot in ((1, 1), (-1, 1 + UP_STEPS)):
            for h in (0, 1):
                first_sends.append(
                    remote(
                        own_piece(a, h),
                        dst.at[slot, c],
                        kv_send.at[a, slot, h],
                        kv_recv.at[a, slot, c],
                        at_z(step, h),
                        x,
                    )
                )
    for copy in first_sends:
        copy.start()

    pltpu.make_async_copy(f_in.at[c], fqbuf.at[me8], local_sem.at[4]).start()

    def q_copies(r):
        to = (me8 + r) % 8
        return (
            remote(f_in.at[to % 2], fqbuf.at[me8], q_send.at[1, r], q_recv.at[1, r], zbase + to, x),
            remote(q_in.at[to % 2], qbuf.at[me8], q_send.at[0, r], q_recv.at[0, r], zbase + to, x),
        )

    def start_q(i, _):
        for copy in q_copies(i + 1):
            copy.start()
        return 0

    lax.fori_loop(0, 7, start_q, 0)

    mine = w_in.shape[0] // 2
    shared_rows = mine // 4
    part = shared_rows // NY
    direct = mine - shared_rows
    eighth = direct // 2
    top_row = c * mine
    rows_a = pl.ds(top_row, direct)
    rows_a0 = pl.ds(top_row, eighth)
    rows_a1 = pl.ds(top_row + eighth, eighth)
    rows_b = pl.ds(top_row + direct, shared_rows)
    across = (x + 2) % NX
    others = (xl, xr, across)

    def share_rows(yy):
        return pl.ds(top_row + direct + yy * part, part)

    def x_of(i, step):
        return (x + step * (1, -1, 2)[i] + NX) % NX

    w_share = [
        remote(
            w_in.at[share_rows(y)], wbuf.at[x, share_rows(y)], w_send.at[i], w_recv.at[i], sp, x_of(i, 1)
        )
        for i in range(3)
    ]
    w_first = [
        remote(w_in.at[rows_a0], wbuf.at[x, rows_a0], w_send.at[3], w_recv.at[3], sp, xr),
        remote(w_in.at[rows_a1], wbuf.at[x, rows_a1], w_send.at[4], w_recv.at[4], sp, xl),
        remote(w_in.at[rows_a1], wbuf.at[x, rows_a1], w_send.at[5], w_recv.at[5], sp, xr),
        remote(w_in.at[rows_a0], wbuf.at[x, rows_a0], w_send.at[6], w_recv.at[6], sp, xl),
    ]
    for copy in w_share + w_first:
        copy.start()
    w_forward = [
        remote(wbuf.at[xl, rows_a0], wbuf.at[xl, rows_a0], w_send.at[7], w_recv.at[7], sp, xr),
        remote(wbuf.at[xr, rows_a1], wbuf.at[xr, rows_a1], w_send.at[8], w_recv.at[8], sp, xl),
    ]
    w_spread = [
        [
            remote(
                wbuf.at[o, share_rows(y)],
                wbuf.at[o, share_rows(y)],
                s_send.at[i, dy],
                s_recv.at[i, dy],
                zbase + ((y + dy) % NY) * 2 + c,
                x,
            )
            for dy in range(1, NY)
        ]
        for i, o in enumerate(others)
    ]
    w_partner = [
        [
            remote(wbuf.at[o, rows], wbuf.at[o, rows], p_send.at[i, k], p_recv.at[i, k], partner, x)
            for k, rows in enumerate((rows_a, rows_b))
        ]
        for i, o in enumerate(others)
    ]
    partner_copies = [copy for row in w_partner for copy in row]
    spread_copies = [copy for row in w_spread for copy in row]

    prepare()

    scale = HEAD_DIM ** (-0.5) * LOG2E
    root = HEAD_DIM**0.5

    def make_bias(slot):
        f0 = fbuf[slot, 0]
        base = f0[:, 0:1]
        for cc in (0, 1):
            rest = (base - (f0 if cc == 0 else fbuf[slot, 1])) * root
            pieces = []
            for _ in range(3):
                piece = rest.astype(jnp.bfloat16).astype(jnp.float32)
                pieces.append(piece)
                rest = rest - piece
            pieces.append(jnp.zeros((104, 256), jnp.float32))
            bias[slot, cc] = jnp.concatenate(pieces, axis=0).T.astype(jnp.bfloat16)

    def score(slot, qb, h, cc):
        q_h = jnp.concatenate([qbuf[qb, h * 128 : (h + 1) * 128, :], ones[h]], axis=0)
        keys = jnp.concatenate([kbuf[slot, cc], bias[slot, cc]], axis=1)
        return jnp.dot(keys, q_h, preferred_element_type=jnp.float32)

    span = 64

    def weigh(slot, qb, h, held):
        delta = (fqbuf[qb, h : h + 1, 0:1] - fbuf[slot, 0, h : h + 1, 0:1]) * root
        pieces = [(cc, slice(r, r + span)) for cc in (0, 1) for r in range(0, 256, span)]
        top = None
        for cc, part in pieces:
            high = jnp.max(held[h, cc, part, :].reshape(span // 8, 8, 256), axis=0)
            top = high if top is None else jnp.maximum(top, high)
        top = jnp.max(top, axis=0, keepdims=True)
        old = stats[qb, h : h + 1, :]
        new = jnp.maximum(old, top + delta)
        shift = new - delta
        factor = jnp.exp2((old - new) * scale)
        total = jnp.zeros((8, 256), jnp.float32)
        p = ([], [])
        for cc, part in pieces:
            e = jnp.exp2((held[h, cc, part, :] - shift) * scale)
            total = total + jnp.sum(e.reshape(span // 8, 8, 256), axis=0)
            p[cc].append(e.astype(jnp.bfloat16))
        total = jnp.sum(total, axis=0, keepdims=True)
        stats[qb, h : h + 1, :] = new
        stats[qb, 2 + h : 3 + h, :] = stats[qb, 2 + h : 3 + h, :] * factor + total
        mixed = jnp.dot(
            vbuf[slot, 0], jnp.concatenate(p[0], axis=0), preferred_element_type=jnp.float32
        ) + jnp.dot(vbuf[slot, 1], jnp.concatenate(p[1], axis=0), preferred_element_type=jnp.float32)
        acc[qb, h] = acc[qb, h] * factor + mixed

    def own_task(qb):
        rows = lax.broadcasted_iota(jnp.int32, (256, 256), 0)
        cols = lax.broadcasted_iota(jnp.int32, (256, 256), 1)
        gap = (qb - 2 * y) * 256
        for h in (0, 1):
            for cc in (0, 1):
                held_a[h, cc] = jnp.where(
                    rows + cc * 256 <= cols + gap, score(0, qb, h, cc), -jnp.inf
                )
        use(held_a, 0, qb)

    def fill(held, slot, qb):
        for h in (0, 1):
            for cc in (0, 1):
                held[h, cc] = score(slot, qb, h, cc)

    def use(held, slot, qb):
        for h in (0, 1):
            weigh(slot, qb, h, held)

    def run_tasks(count, place, after=None):
        @pl.when(count > 0)
        def _():
            fill(held_a, *place(0))

        def pair(i, _):
            first, second = 2 * i, 2 * i + 1
            fill(held_b, *place(second))
            use(held_a, *place(first))
            if after is not None:
                after(first)
            fill(held_a, *place(jnp.minimum(second + 1, count - 1)))
            use(held_b, *place(second))
            if after is not None:
                after(second)
            return 0

        lax.fori_loop(0, count // 2, pair, 0)

    def wait_first(a, slot):
        for h in (0, 1):
            remote(
                own_piece(a, h),
                kv_arrays[a][1].at[slot, h],
                kv_send.at[a, slot, h],
                kv_recv.at[a, slot, h],
                partner,
                x,
            ).wait_recv()

    def forward(a, slot, step):
        buf = kv_arrays[a][1]
        if slot in (UP_STEPS - 1, UP_STEPS + DOWN_STEPS):
            piece = 0 if slot == UP_STEPS - 1 else 1
            return remote(
                buf.at[slot, piece],
                buf.at[UP_STEPS, piece],
                kv_send.at[a, UP_STEPS, piece],
                kv_recv.at[a, UP_STEPS, piece],
                at_z(step, c),
                x,
            )
        return remote(
            buf.at[slot],
            buf.at[slot + 1],
            kv_send.at[a, slot + 1, 0],
            kv_recv.at[a, slot + 1, 0],
            at_z(step, c),
            x,
        )

    forwards = []

    def arrive(slot, step, first, send_on):
        for a in (2, 0, 1):
            if first:
                wait_first(a, slot)
            else:
                forward(a, slot - 1, step).wait_recv()
            if send_on:
                copy = forward(a, slot, step)
                copy.start()
                forwards.append(copy)

    def valid(j):
        return jnp.where(z >= j, 1, 0) + jnp.where(z >= NZ - j, 1, 0)

    def peer(i):
        return jnp.where(i % 2 == 1, (i + 1) // 2, (8 - i // 2) % 8)

    def block_of(i):
        return (me8 + 8 - peer(i)) % 8

    def wait_query(i):
        @pl.when(i > 0)
        def _():
            for copy in q_copies(jnp.maximum(peer(i), 1)):
                copy.wait_recv()

    def own(i):
        wait_query(i)
        qb = block_of(i)

        @pl.when(qb // 2 >= y)
        def _():
            own_task(qb)

    for a in range(3):
        pltpu.make_async_copy(own_piece(a, c), kv_arrays[a][1].at[0, c], local_sem.at[a]).wait()
        remote(
            own_piece(a, 1 - c),
            kv_arrays[a][1].at[0, c],
            kv_send.at[a, 0, 0],
            kv_recv.at[a, 0, 0],
            partner,
            x,
        ).wait_recv()
    pltpu.make_async_copy(q_in.at[c], qbuf.at[me8], local_sem.at[3]).wait()
    pltpu.make_async_copy(f_in.at[c], fqbuf.at[me8], local_sem.at[4]).wait()
    make_bias(0)

    near = 4

    def stage_a(i, _):
        own(i)
        return 0

    lax.fori_loop(0, near, stage_a, 0)
    arrive(1, 1, True, True)
    arrive(5, -1, True, True)
    for i in range(3):
        w_share[i].wait_recv()
        for copy in w_spread[i]:
            copy.start()
    make_bias(1)
    make_bias(5)

    run_tasks(near * valid(1), lambda t: (1 + 4 * (t // near), block_of(t % near)))
    arrive(2, 1, False, True)
    arrive(6, -1, False, True)
    make_bias(2)
    make_bias(6)
    w_first[0].wait_recv()
    w_forward[0].start()
    w_first[1].wait_recv()
    w_forward[1].start()

    lax.fori_loop(near, 8, stage_a, 0)
    run_tasks(near * valid(1), lambda t: (1 + 4 * (t // near), block_of(near + t % near)))
    arrive(3, 1, False, True)
    arrive(7, -1, False, True)
    make_bias(3)
    make_bias(7)
    run_tasks(8 * valid(2), lambda t: (2 + 4 * (t // 8), block_of(t % 8)))
    w_first[2].wait_recv()
    w_first[3].wait_recv()
    w_partner[0][0].start()
    w_partner[1][0].start()
    run_tasks(8 * valid(3), lambda t: (3 + 4 * (t // 8), block_of(t % 8)))
    w_forward[0].wait_recv()
    w_forward[1].wait_recv()
    w_partner[2][0].start()
    for a in (2, 0, 1):
        forward(a, 3, 1).wait_recv()
        forward(a, 7, -1).wait_recv()
    make_bias(4)

    def o_copy(r8, rx):
        to = (me8 + r8) % 8
        tx = (x + rx) % NX
        return (
            remote(
                obuf.at[to, pl.ds(tx * 64, 64)],
                rbuf.at[y, x * 2 + c],
                o_send.at[r8, rx],
                o_recv.at[r8, rx],
                zbase + to,
                tx,
            ),
            remote(
                lbuf.at[to, tx // 2],
                lrecv.at[y, x * 2 + c],
                l_send.at[r8, rx],
                l_recv.at[r8, rx],
                zbase + to,
                tx,
            ),
        )

    def finish(r):
        i = 7 - r
        qb = block_of(i)
        r8 = (8 - peer(i)) % 8
        sums = []
        for h in (0, 1):
            total = stats[qb, 2 + h : 3 + h, :]
            some = total > 0.0
            inv = jnp.where(some, 1.0 / jnp.where(some, total, 1.0), 0.0)
            obuf[qb, :, h * 128 : (h + 1) * 128] = (acc[qb, h] * inv).T.astype(jnp.bfloat16)
            sums.append(
                jnp.where(
                    some, stats[qb, h : h + 1, :] * scale + jnp.log2(jnp.where(some, total, 1.0)), NEG
                )
            )
        both = jnp.concatenate(sums + [jnp.zeros((6, 256), jnp.float32)], axis=0)
        lbuf[qb, 0] = both[:, :128]
        lbuf[qb, 1] = both[:, 128:]
        for rx in (2, 1, 3):
            for copy in o_copy(r8, rx):
                copy.start()

        @pl.when(r8 > 0)
        def _():
            for copy in o_copy(r8, 0):
                copy.start()

    last = jnp.where(z >= UP_STEPS, 1, 0)

    def last_place(t):
        return UP_STEPS, block_of(7 - t)

    def leave(t):
        finish(t)

    run_tasks(8 * last, last_place, leave)

    def finish_early(r, _):
        finish(r)
        return 0

    lax.fori_loop(0, jnp.where(last == 0, 8, 0), finish_early, 0)
    for copy in spread_copies:
        copy.wait_recv()
    for row in w_partner:
        row[1].start()
    own_copies = (
        pltpu.make_async_copy(
            obuf.at[me8, pl.ds(x * 64, 64)],
            rbuf.at[y, x * 2 + c],
            local_sem.at[6],
        ),
        pltpu.make_async_copy(lbuf.at[me8, x // 2], lrecv.at[y, x * 2 + c], local_sem.at[7]),
    )
    for copy in own_copies:
        copy.start()
    for copy in own_copies:
        copy.wait()

    def wait_o(r, _):
        for copy in o_copy((r + 1) // NX, (r + 1) % NX):
            copy.wait_recv()
        return 0

    lax.fori_loop(0, 31, wait_o, 0)

    logs = [lrecv[i].reshape(64, 128) for i in range(NY)]
    top = jnp.maximum(jnp.maximum(logs[0], logs[1]), jnp.maximum(logs[2], logs[3]))
    parts = [jnp.exp2(v - top) for v in logs]
    inv = 1.0 / (parts[0] + parts[1] + parts[2] + parts[3])
    for i in range(NY):
        scaled = parts[i] * inv
        wcols[i] = jnp.concatenate([scaled, scaled], axis=0).T
    first_row = pl.multiple_of((x % 2) * 64, 64)
    shares = [wcols[i, pl.ds(first_row, 64), :] for i in range(NY)]
    for n in range(HEADS):
        lane = (n // 2) * 8 + n % 2
        cols = slice(n * 128, (n + 1) * 128)
        half = slice(n % 2 * 128, n % 2 * 128 + 128)
        mixed = shares[0][:, lane : lane + 1] * rbuf[0, n // 2, :, half].astype(jnp.float32)
        for i in range(1, NY):
            mixed = mixed + shares[i][:, lane : lane + 1] * rbuf[i, n // 2, :, half].astype(
                jnp.float32
            )
        att[:, cols] = mixed.astype(jnp.bfloat16)

    pltpu.make_async_copy(w_in, wbuf.at[x], local_sem.at[5]).wait()
    pltpu.make_async_copy(res_in, res_ref, local_sem.at[8]).wait()
    pltpu.make_async_copy(gain_in, gain_ref, local_sem.at[9]).wait()
    for copy in partner_copies:
        copy.wait_recv()

    width = w_in.shape[1]
    chunk = 256

    def project(i, total):
        cols = pl.ds(pl.multiple_of(i * chunk, chunk), chunk)
        part = jnp.dot(att[:, 0:512], wbuf[0, :, cols], preferred_element_type=jnp.float32)
        for b in range(1, NX):
            part = part + jnp.dot(
                att[:, b * 512 : (b + 1) * 512],
                wbuf[b, :, cols],
                preferred_element_type=jnp.float32,
            )
        stream = (res_ref[:, cols].astype(jnp.float32) + part).astype(jnp.bfloat16)
        stream_ref[:, cols] = stream
        wide = stream.astype(jnp.float32)
        return total + jnp.sum(wide * wide, axis=1, keepdims=True)

    total = lax.fori_loop(0, width // chunk, project, jnp.zeros((64, 1), jnp.float32))
    rate = lax.rsqrt(total * (1.0 / width) + norm_eps)
    normed_ref[...] = (stream_ref[...].astype(jnp.float32) * rate * gain_ref[...]).astype(
        jnp.bfloat16
    )

    for copy in first_sends + forwards + w_share + w_first + w_forward + spread_copies + partner_copies:
        copy.wait_send()

    def wait_q(i, _):
        for copy in q_copies(i + 1):
            copy.wait_send()
        return 0

    lax.fori_loop(0, 7, wait_q, 0)

    def wait_sent(r, _):
        for copy in o_copy((r + 1) // NX, (r + 1) % NX):
            copy.wait_send()
        return 0

    lax.fori_loop(0, 31, wait_sent, 0)


def experts_parts(
    normed_ref,
    stream_ref,
    ids_ref,
    route_ref,
    eg_in,
    eu_in,
    ed_in,
    sg_in,
    su_in,
    sd_in,
    out_ref,
    nbuf,
    table,
    tables,
    sel,
    gate,
    sbuf,
    xbuf,
    obuf,
    rbuf,
    cin,
    cout,
    total,
    eg,
    eu,
    ed,
    sg,
    su,
    sd,
    n_send,
    n_recv,
    t_send,
    t_recv,
    x_send,
    x_recv,
    r_send,
    r_recv,
    c_send,
    c_recv,
    w_sem,
    x_sem,
    r_sem,
):
    sp = lax.axis_index("sp")
    x = lax.axis_index("tp")
    z = sp // 8
    me8 = sp % 8
    zbase = z * 8
    width = normed_ref.shape[1]
    half = width // 2

    def at_z(step):
        return ((z + step + NZ) % NZ) * 8 + me8

    loads = [
        pltpu.make_async_copy(src, dst, w_sem.at[i])
        for i, (src, dst) in enumerate(
            (
                (sg_in, sg),
                (su_in, su),
                (sd_in, sd),
                (eg_in.at[0], eg),
                (eu_in.at[0], eu),
                (ed_in.at[0], ed),
            )
        )
    ]
    def remote(src, dst, send, recv, sp_id):
        return pltpu.make_async_remote_copy(
            src_ref=src,
            dst_ref=dst,
            send_sem=send,
            recv_sem=recv,
            device_id=(sp_id, x),
            device_id_type=MESH,
        )

    def pass_on(slot, to_slot, hf, step):
        return remote(
            nbuf.at[slot, hf],
            nbuf.at[to_slot, hf],
            n_send.at[to_slot, hf],
            n_recv.at[to_slot, hf],
            at_z(step),
        )

    sent = []

    def send(copy):
        copy.start()
        sent.append(copy)

    f32, bf16 = jnp.float32, jnp.bfloat16
    up, down = 1, 1 + UP_STEPS

    def table_copy(r):
        to = (z + r) % NZ
        return remote(table.at[to], tables.at[z], t_send.at[r], t_recv.at[r], to * 8 + me8)

    def prepare():
        for copy in loads:
            copy.start()

        both = jnp.concatenate([ids_ref[...].astype(f32), route_ref[...]], axis=0)
        both = jnp.concatenate([both, jnp.zeros_like(both)], axis=1)
        columns = jnp.concatenate([both] * 16, axis=0).T
        rows = ids_ref.shape[1]
        ids = columns[:rows, :TOPK]
        weights = columns[:rows, TOPK : 2 * TOPK]
        gates = weights / jnp.sum(weights, axis=1, keepdims=True) * routed_scale
        experts = lax.broadcasted_iota(jnp.int32, (rows, 64), 1).astype(f32)
        named = jnp.zeros((rows, 64), f32)
        shares = jnp.zeros((rows, 64), f32)
        for k in range(TOPK):
            hit = ids[:, k : k + 1] == experts
            named = named + jnp.where(hit, 1.0, 0.0)
            shares = shares + jnp.where(hit, gates[:, k : k + 1], 0.0)
        earlier = (
            lax.broadcasted_iota(jnp.int32, (rows, rows), 1)
            < lax.broadcasted_iota(jnp.int32, (rows, rows), 0)
        )
        named = named.astype(bf16)
        rank = jnp.dot(jnp.where(earlier, 1.0, 0.0).astype(bf16), named, preferred_element_type=f32)
        lane = lax.broadcasted_iota(jnp.int32, (64, 1024), 1)
        expert = lax.broadcasted_iota(jnp.int32, (64, 1024), 0)
        spread = jnp.where(lane // 16 == expert, 1.0, 0.0).astype(bf16)
        named_x = jnp.dot(named, spread, preferred_element_type=f32)
        rank_x = jnp.dot(rank.astype(bf16), spread, preferred_element_type=f32)
        share_x = jnp.dot(shares.astype(bf16), spread, preferred_element_type=f32)
        want = (lax.broadcasted_iota(jnp.int32, (rows, 1024), 1) % 8).astype(f32)
        filled = jnp.where(rank_x == want, named_x, 0.0)
        token = lax.broadcasted_iota(jnp.int32, (rows, 1024), 0).astype(f32)
        source = jnp.sum(filled * (token + 1000.0), axis=0, keepdims=True) - 1000.0
        share = jnp.sum(filled * share_x, axis=0, keepdims=True)
        for p in range(NZ):
            lanes = slice(p * 128, (p + 1) * 128)
            table[p] = jnp.concatenate(
                [source[:, lanes], share[:, lanes], jnp.zeros((6, 128), f32)], axis=0
            )
        tables[z] = table[z]

        for r in range(1, NZ):
            send(table_copy(r))

    def main():
        nbuf[0, 0] = normed_ref[:, :half]
        nbuf[0, 1] = normed_ref[:, half:]
        for hf in (0, 1):
            send(pass_on(0, up, hf, 1))
            send(pass_on(0, down, hf, -1))

        for copy in loads[:3]:
            copy.wait()
        n = normed_ref[...]
        g = jnp.dot(n, sg[...], preferred_element_type=f32)
        u = jnp.dot(n, su[...], preferred_element_type=f32)
        hidden = (g / (1.0 + jnp.exp(-g)) * u).astype(bf16)
        for i in range(4):
            cols = slice(i * width // 4, (i + 1) * width // 4)
            total[:, cols] = stream_ref[:, cols].astype(f32) + jnp.dot(
                hidden, sd[:, cols], preferred_element_type=f32
            )

        pairs = ((1, 5), (2, 6), (3, 7), (4, 0))
        offset = {0: 0, 1: -1, 2: -2, 3: -3, 4: -4, 5: 1, 6: 2, 7: 3}

        def arrive(slot, step, send_on, hf):
            if slot == UP_STEPS:
                pass_on(3 if hf == 0 else 7, slot, hf, 1 if hf == 0 else -1).wait_recv()
                return
            pass_on(slot - 1 if slot not in (up, down) else 0, slot, hf, step).wait_recv()
            if slot in (3, 7):
                if hf == (0 if slot == 3 else 1):
                    send(pass_on(slot, UP_STEPS, hf, step))
            elif send_on:
                send(pass_on(slot, slot + 1, hf, step))

        def x_copy(b, hf, r):
            to = (me8 + r) % 8
            return remote(
                sbuf.at[b, hf, to], xbuf.at[b, hf, me8], x_send.at[b, hf, r], x_recv.at[b, hf, r], zbase + to
            )

        def r_copy(b, hf, r):
            to = (me8 + r) % 8
            return remote(
                obuf.at[b, hf, to], rbuf.at[b, hf, me8], r_send.at[b, hf, r], r_recv.at[b, hf, r], zbase + to
            )

        def x_own(b, hf):
            return pltpu.make_async_copy(sbuf.at[b, hf, me8], xbuf.at[b, hf, me8], x_sem.at[b, hf])

        def r_own(b, hf):
            return pltpu.make_async_copy(obuf.at[b, hf, me8], rbuf.at[b, hf, me8], r_sem.at[b, hf])

        def choose(b):
            first, second = pairs[b]
            ta = tables[(z + offset[first] + NZ) % NZ]
            tb = tables[(z + offset[second] + NZ) % NZ]
            lane_of = lax.broadcasted_iota(jnp.int32, (1, 128), 1) % 16
            src = jnp.where(lane_of < 8, ta[0:1], tb[0:1] + 64.0)
            share_row = jnp.where(lane_of < 8, ta[1:2], tb[1:2])
            token_of = lax.broadcasted_iota(jnp.int32, (128, 128), 0).astype(f32)
            chosen = jnp.where(token_of == src, 1.0, 0.0)
            sel[...] = chosen.T.astype(bf16)
            gate[b] = (chosen * share_row).astype(bf16)

        def dispatch(b, hf):
            first, second = pairs[b]
            for i in range(2):
                cols = slice(i * half // 2, (i + 1) * half // 2)
                tokens = jnp.concatenate([nbuf[first, hf, :, cols], nbuf[second, hf, :, cols]], axis=0)
                picked = jnp.dot(sel[...], tokens, preferred_element_type=f32)
                sbuf[b, hf, :, :, cols] = picked.astype(bf16).reshape(8, 16, half // 2)
            for r in (4, 3, 5, 2, 6, 1, 7):
                send(x_copy(b, hf, r))
            x_own(b, hf).start()

        def give_back(b, hf):
            for r in (4, 3, 5, 2, 6, 1, 7):
                send(r_copy(b, hf, r))
            r_own(b, hf).start()

        def run_expert(b, give):
            g = u = None
            for hf in (0, 1):
                for r in range(1, 8):
                    x_copy(b, hf, r).wait_recv()
                x_own(b, hf).wait()
                rows_in = xbuf[b, hf].reshape(128, half)
                deep = slice(hf * half, (hf + 1) * half)
                g_part = jnp.dot(rows_in, eg[deep, :], preferred_element_type=f32)
                u_part = jnp.dot(rows_in, eu[deep, :], preferred_element_type=f32)
                g = g_part if g is None else g + g_part
                u = u_part if u is None else u + u_part
            hidden = (g / (1.0 + jnp.exp(-g)) * u).astype(bf16)
            for hf in (0, 1):
                for i in range(2):
                    cols = slice(i * half // 2, (i + 1) * half // 2)
                    at = hf * half + i * half // 2
                    made = jnp.dot(hidden, ed[:, at : at + half // 2], preferred_element_type=f32)
                    obuf[b, hf, :, :, cols] = made.astype(bf16).reshape(8, 16, half // 2)
                if give:
                    give_back(b, hf)

        def need_tables(*steps):
            for r in steps:
                table_copy(r).wait_recv()

        for b, moves, steps in (
            (0, ((1, 1, True), (5, -1, True)), (1, 7)),
            (1, ((2, 1, True), (6, -1, True)), (2, 6)),
            (2, ((3, 1, True), (7, -1, True)), (3, 5)),
            (3, ((4, 1, False),), (4,)),
        ):
            for hf in (0, 1):
                for slot, step, send_on in moves:
                    arrive(slot, step, send_on, hf)
                if hf == 0:
                    need_tables(*steps)
                    choose(b)
                dispatch(b, hf)
            if b == 0:
                for copy in loads[3:]:
                    copy.wait()
            else:
                run_expert(b - 1, False)
        run_expert(3, True)
        for b in (2, 1, 0):
            for hf in (0, 1):
                give_back(b, hf)

        def chain_copy(way, place, hf):
            return remote(
                cout.at[way, place, hf],
                cin.at[way, place, hf],
                c_send.at[way, place, hf],
                c_recv.at[way, place, hf],
                at_z(-1 if way == 0 else 1),
            )

        for b, places in ((3, (3, None)), (2, (2, 2)), (1, (1, 1)), (0, (0, 0))):
            for hf in (0, 1):
                for r in range(1, 8):
                    r_copy(b, hf, r).wait_recv()
                r_own(b, hf).wait()
                cols = slice(hf * half, (hf + 1) * half)
                part = jnp.dot(
                    gate[b], rbuf[b, hf].reshape(128, half), preferred_element_type=f32
                )
                for way in (0, 1):
                    mine = part[way * 64 : (way + 1) * 64]
                    place = places[way]
                    if place is None:
                        total[:, cols] = total[:, cols] + mine
                        continue
                    side = way if place < 3 else hf
                    if place < 2 or (place == 2 and hf == way):
                        chain_copy(side, place + 1, hf).wait_recv()
                        mine = mine + cin[side, place + 1, hf].astype(f32)
                    cout[side, place, hf] = mine.astype(bf16)
                    send(chain_copy(side, place, hf))
        for hf in (0, 1):
            cols = slice(hf * half, (hf + 1) * half)
            for way in (0, 1):
                chain_copy(way, 0, hf).wait_recv()
            out_ref[:, cols] = (
                total[:, cols] + cin[0, 0, hf].astype(f32) + cin[1, 0, hf].astype(f32)
            ).astype(bf16)
        for copy in sent:
            copy.wait_send()

    return prepare, main


def layer_kernel(*refs):
    att_in, (ids, route), weights = refs[:7], refs[7:9], refs[9:15]
    out, stream, normed = refs[15:18]
    att_scratch, scratch = refs[18 : 18 + ATTENTION_SCRATCH], refs[18 + ATTENTION_SCRATCH :]
    prepare, main = experts_parts(normed, stream, ids, route, *weights, out, *scratch)
    attention_kernel(prepare, *att_in, stream, normed, *att_scratch)
    main()


ATTENTION_SCRATCH = 36


def layer(
    residual,
    queries,
    key_rows,
    value_rows,
    forget_sums,
    out_weight,
    norm_gain,
    expert_ids,
    route_weights,
    expert_gate,
    expert_up,
    expert_down,
    shared_gate,
    shared_up,
    shared_down,
):
    rows, width = residual.shape
    tokens = queries.shape[0]
    hidden = expert_gate.shape[2]
    shared = shared_gate.shape[1]
    q_in = queries.T.reshape(2, 256, tokens)
    v_in = value_rows.T.reshape(2, 128, tokens)
    bf16, f32 = jnp.bfloat16, jnp.float32
    anywhere = pl.BlockSpec(memory_space=pl.ANY)
    vmem = pl.BlockSpec(memory_space=pltpu.VMEM)
    dma = pltpu.SemaphoreType.DMA
    return pl.pallas_call(
        layer_kernel,
        out_shape=jax.ShapeDtypeStruct((rows, width), bf16),
        in_specs=[anywhere, anywhere, anywhere, vmem] + [anywhere] * 3 + [vmem] * 2 + [anywhere] * 6,
        out_specs=vmem,
        scratch_shapes=[
            pltpu.VMEM((rows, width), bf16),
            pltpu.VMEM((rows, width), bf16),
            pltpu.VMEM((8, 256, 256), bf16),
            pltpu.VMEM((8, 8, 256), f32),
            pltpu.VMEM((8, 2, 256, 128), bf16),
            pltpu.VMEM((8, 2, 128, 256), bf16),
            pltpu.VMEM((8, 2, 8, 256), f32),
            pltpu.VMEM((2, 8, 256), f32),
            pltpu.VMEM((8, 2, 256, 128), bf16),
            pltpu.VMEM((2, 128, 256), bf16),
            pltpu.VMEM((2, 2, 256, 256), f32),
            pltpu.VMEM((2, 2, 256, 256), f32),
            pltpu.VMEM((64, 2048), bf16),
            pltpu.VMEM((1, 2048), f32),
            pltpu.VMEM((8, 2, 128, 256), f32),
            pltpu.VMEM((8, 8, 256), f32),
            pltpu.VMEM((8, 256, 256), bf16),
            pltpu.VMEM((8, 2, 8, 128), f32),
            pltpu.VMEM((4, 8, 64, 256), bf16),
            pltpu.VMEM((4, 8, 8, 128), f32),
            pltpu.VMEM((4, 128, 128), f32),
            pltpu.VMEM((64, 2048), bf16),
            pltpu.VMEM((4, 512, 2048), bf16),
            dma((2, 8)),
            dma((2, 8)),
            dma((3, 8, 2)),
            dma((3, 8, 2)),
            dma((8, 4)),
            dma((8, 4)),
            dma((8, 4)),
            dma((8, 4)),
            dma((9,)),
            dma((9,)),
            dma((3, NY)),
            dma((3, NY)),
            dma((3, 2)),
            dma((3, 2)),
            dma((10,)),
            pltpu.VMEM((8, 2, rows, width // 2), bf16),
            pltpu.VMEM((8, 8, 128), f32),
            pltpu.VMEM((8, 8, 128), f32),
            pltpu.VMEM((128, 128), bf16),
            pltpu.VMEM((4, 128, 128), bf16),
            pltpu.VMEM((4, 2, 8, 16, width // 2), bf16),
            pltpu.VMEM((4, 2, 8, 16, width // 2), bf16),
            pltpu.VMEM((4, 2, 8, 16, width // 2), bf16),
            pltpu.VMEM((4, 2, 8, 16, width // 2), bf16),
            pltpu.VMEM((2, 4, 2, rows, width // 2), bf16),
            pltpu.VMEM((2, 4, 2, rows, width // 2), bf16),
            pltpu.VMEM((rows, width), f32),
            pltpu.VMEM((width, hidden), bf16),
            pltpu.VMEM((width, hidden), bf16),
            pltpu.VMEM((hidden, width), bf16),
            pltpu.VMEM((width, shared), bf16),
            pltpu.VMEM((width, shared), bf16),
            pltpu.VMEM((shared, width), bf16),
            dma((8, 2)),
            dma((8, 2)),
            dma((8,)),
            dma((8,)),
            dma((4, 2, 8)),
            dma((4, 2, 8)),
            dma((4, 2, 8)),
            dma((4, 2, 8)),
            dma((2, 4, 2)),
            dma((2, 4, 2)),
            dma((6,)),
            dma((4, 2)),
            dma((4, 2)),
        ],
        compiler_params=pltpu.CompilerParams(
            collective_id=0, has_side_effects=True, vmem_limit_bytes=66_000_000
        ),
        cost_estimate=pl.CostEstimate(
            flops=12 * 10**9, bytes_accessed=32 * 2**20, transcendentals=16 * 2**20
        ),
    )(
        q_in,
        key_rows,
        v_in,
        forget_sums.T,
        out_weight,
        residual,
        norm_gain.reshape(1, width),
        expert_ids.T,
        route_weights.T,
        expert_gate,
        expert_up,
        expert_down,
        shared_gate,
        shared_up,
        shared_down,
    )


def solution(mesh):
    in_specs = (
        P(("sp", "tp"), None),
        P("sp", "tp"),
        P("sp", "tp"),
        P("sp", "tp"),
        P("sp", "tp"),
        P("tp", None),
        P(),
        P(("sp", "tp"), None),
        P(("sp", "tp"), None),
        P("sp", None, None),
        P("sp", None, None),
        P("sp", None, None),
        P(),
        P(),
        P(),
    )
    out_specs = P(("sp", "tp"), None)
    return jax.shard_map(layer, mesh=mesh, in_specs=in_specs, out_specs=out_specs, check_vma=False)
```

time: 151 us -> 141 us (0.934)
  Pallas kernels: 143 us -> 135 us
    pallas_call x2 -> x1, Pallas kernels: 143 us -> 135 us  [layer(): pl.pallas_call(layer_kernel, out_shape=jax.ShapeDtypeStruct((rows, width)...]
    unnamed x7 -> x1, local copies, waits for them, and re-layouts: 3.09 us -> 1.67 us
where the time goes in v4:
time: 141 us; the launch traced here: 140 us
  Pallas kernels  135 us (96%)
  local copies, waits for them, and re-layouts  5.13 us (4%)
    pallas_call x1, Pallas kernels, layer(): pl.pallas_call(layer_kernel, out_shape=jax.ShapeDtypeStruct((rows, width)...  135 us

profile of v4, /device:TPU:8, one launch (start us, length us, event | category | flops | bytes accessed | tf_op | source)
XLA Modules:
  0.0 139.9 jit_solution(11676570145128503836)
XLA Ops:
  0.0 1.7 %copy.17 = bf16[256,256]{1,0:T(8,128)(2,1)} copy(bf16[256,256]{0,1:T(8,128)(2,1)} %bitcast.10) | data formatting | bytes 262144 | tf_op jit(solution)/shard_map/transpose | solution.py:968
  1.7 1.8 %copy.16 = bf16[512,256]{1,0:T(8,128)(2,1)} copy(bf16[512,256]{0,1:T(8,128)(2,1)} %bitcast.8) | data formatting | bytes 524288 | tf_op jit(solution)/shard_map/transpose | solution.py:967
  3.5 134.8 %shard_map.145 = bf16[64,2048]{1,0:T(8,128)(2,1)} custom-call(bf16[2,256,256]{2,1,0:T(8,128)(2,1)} %bitcast.9, bf16[256,256]{1,0:T(8,128)(2,1)} %refs_1_.1, bf16[2,128,256]{2,1,0:T(8,128)(2,1)} %bitcast.11, f32[4,256]{1,0:T(4,128)} %bitcast.13, bf16[512,2048]{1,0:T(8,128)(2,1)} %refs_4_.1, bf16[64,2048]{1,0:T(8,128)(2,1)} %refs_5_.1, f32[1,2048]{1,0:T(1,128)} %bitcast.12, ...), custom_call_target="tpu_custom_call" | custom-call | flops 12000000000 | bytes 33554432 | tf_op jit(solution)/shard_map/pallas_call | solution.py:973
  138.2 1.7 %copy.19 = bf16[64,2048]{1,0:T(8,128)(2,1)} copy(bf16[64,2048]{1,0:T(8,128)(2,1)} %shard_map.145) | data formatting | bytes 524288

commit v5 on v4

--- a/solution.py
+++ b/solution.py
@@ -22,15 +22,17 @@
 
 def attention_kernel(
     prepare,
-    q_in,
+    q_rows,
     k_rows,
-    v_in,
+    v_rows,
     f_rows,
     w_in,
     res_in,
     gain_in,
     stream_ref,
     normed_ref,
+    q_in,
+    v_in,
     qbuf,
     fqbuf,
     kbuf,
@@ -104,11 +106,12 @@
             pl.semaphore_signal(
                 barrier, inc=1, device_id=(at_z(step, core), x), device_id_type=MESH
             )
-    pltpu.make_async_copy(q_in.at[c], qbuf.at[me8], local_sem.at[3]).start()
     pltpu.make_async_copy(w_in, wbuf.at[x], local_sem.at[5]).start()
     pltpu.make_async_copy(res_in, res_ref, local_sem.at[8]).start()
     pltpu.make_async_copy(gain_in, gain_ref, local_sem.at[9]).start()
     for h in (0, 1):
+        q_in[h] = q_rows[:, h * 256 : (h + 1) * 256].T
+        v_in[h] = v_rows[:, h * 128 : (h + 1) * 128].T
         f_in[h] = jnp.concatenate(
             [f_rows[2 * h : 2 * h + 2, :], jnp.zeros((6, f_rows.shape[1]), jnp.float32)], axis=0
         )
@@ -165,6 +168,7 @@
     for copy in first_sends:
         copy.start()
 
+    pltpu.make_async_copy(q_in.at[c], qbuf.at[me8], local_sem.at[3]).start()
     pltpu.make_async_copy(f_in.at[c], fqbuf.at[me8], local_sem.at[4]).start()
 
     def q_copies(r):
@@ -940,7 +944,7 @@
     main()
 
 
-ATTENTION_SCRATCH = 36
+ATTENTION_SCRATCH = 38
 
 
 def layer(
@@ -964,8 +968,6 @@
     tokens = queries.shape[0]
     hidden = expert_gate.shape[2]
     shared = shared_gate.shape[1]
-    q_in = queries.T.reshape(2, 256, tokens)
-    v_in = value_rows.T.reshape(2, 128, tokens)
     bf16, f32 = jnp.bfloat16, jnp.float32
     anywhere = pl.BlockSpec(memory_space=pl.ANY)
     vmem = pl.BlockSpec(memory_space=pltpu.VMEM)
@@ -973,11 +975,13 @@
     return pl.pallas_call(
         layer_kernel,
         out_shape=jax.ShapeDtypeStruct((rows, width), bf16),
-        in_specs=[anywhere, anywhere, anywhere, vmem] + [anywhere] * 3 + [vmem] * 2 + [anywhere] * 6,
+        in_specs=[vmem] * 4 + [anywhere] * 3 + [vmem] * 2 + [anywhere] * 6,
         out_specs=vmem,
         scratch_shapes=[
             pltpu.VMEM((rows, width), bf16),
             pltpu.VMEM((rows, width), bf16),
+            pltpu.VMEM((2, 256, tokens), bf16),
+            pltpu.VMEM((2, 128, tokens), bf16),
             pltpu.VMEM((8, 256, 256), bf16),
             pltpu.VMEM((8, 8, 256), f32),
             pltpu.VMEM((8, 2, 256, 128), bf16),
@@ -1053,9 +1057,9 @@
             flops=12 * 10**9, bytes_accessed=32 * 2**20, transcendentals=16 * 2**20
         ),
     )(
-        q_in,
+        queries,
         key_rows,
-        v_in,
+        value_rows,
         forget_sums.T,
         out_weight,
         residual,

time: 141 us -> 138 us (0.979)
  local copies, waits for them, and re-layouts: 5.13 us -> 1.67 us
    transpose x2 -> x0, local copies, waits for them, and re-layouts: 3.46 us -> none  [the longest x1 1.79 us: layer(): q_in = queries.T.reshape(2, 256, tokens)]
where the time goes in v5:
time: 138 us; the launch traced here: 137 us
  Pallas kernels  136 us (99%)
  local copies, waits for them, and re-layouts  1.67 us (1%)
    pallas_call x1, Pallas kernels, layer(): pl.pallas_call(layer_kernel, out_shape=jax.ShapeDtypeStruct((rows, width)...  136 us

profile of v5, /device:TPU:8, one launch (start us, length us, event | category | flops | bytes accessed | tf_op | source)
XLA Modules:
  0.0 137.3 jit_solution(3234867951353518275)
XLA Ops:
  0.0 135.6 %shard_map.145 = bf16[64,2048]{1,0:T(8,128)(2,1)} custom-call(bf16[256,512]{1,0:T(8,128)(2,1)} %refs_0_.1, bf16[256,256]{1,0:T(8,128)(2,1)} %refs_1_.1, bf16[256,256]{1,0:T(8,128)(2,1)} %refs_2_.1, f32[4,256]{1,0:T(4,128)} %bitcast.5, bf16[512,2048]{1,0:T(8,128)(2,1)} %refs_4_.1, bf16[64,2048]{1,0:T(8,128)(2,1)} %refs_5_.1, f32[1,2048]{1,0:T(1,128)} %bitcast.4, ...), custom_call_target="tpu_custom_call" | custom-call | flops 12000000000 | bytes 33554432 | tf_op jit(solution)/shard_map/pallas_call | solution.py:975
  135.6 1.7 %copy.17 = bf16[64,2048]{1,0:T(8,128)(2,1)} copy(bf16[64,2048]{1,0:T(8,128)(2,1)} %shard_map.145) | data formatting | bytes 524288
